TPU v7x, 32 devices: a whole 2x2x4 slice. The times are simulated.
32 devices in a mesh: ep: 8 (over z, x), tp: 4 (over y, core).
Axes of the slice: x: 2, y: 2, z: 4, core: 2. Of those that a mesh axis runs over, the one named last changes fastest.
Arguments:
- tokens: bfloat16 [1024, 2048], P('ep', 'tp'), may hold values from -6 to 6
- cotangent: bfloat16 [1024, 2048], P('ep', 'tp'), may hold values from -6 to 6
- experts: int32 [1024, 2], P('ep'), may hold values from 0 to 7, as said below
- combine: float32 [1024, 2], P('ep'), may hold values from 0.2 to 1
- w_gate: bfloat16 [8, 2048, 256], P('ep', 'tp'), may hold values from -0.125 to 0.125
- w_up: bfloat16 [8, 2048, 256], P('ep', 'tp'), may hold values from -0.125 to 0.125
- w_down: bfloat16 [8, 256, 2048], P('ep', None, 'tp'), may hold values from -0.375 to 0.375
Outputs:
- grad_tokens: bfloat16 [1024, 2048], P('ep', 'tp')
- grad_combine: float32 [1024, 2], P('ep')
- gate_grad: float32 [8, 2048, 256], P('ep', 'tp')
- up_grad: float32 [8, 2048, 256], P('ep', 'tp')
- down_grad: float32 [8, 256, 2048], P('ep', None, 'tp')
Inputs may be any that keep to these rules, and one draw needn't show every extreme that they name: Each row names two different experts of one group of 4 consecutive experts. The rows of one index of ep name any one expert at most 64 times, and some expert exactly 64 times.
All inputs are finite; a program needn't handle non-finite values.
Results may differ from a plain program's by a relative error of at most 0.019.
Values may be sent and summed in bfloat16 or wider, within the bound.
A program may use at most 64 MiB of HBM per device.

v0:
```python
import functools

import jax
import jax.numpy as jnp
from jax import lax
from jax.experimental import pallas as pl
from jax.experimental.pallas import tpu as pltpu
from jax.sharding import PartitionSpec as P


def slot_positions(routed, total_experts, capacity):
    onehot = (routed[:, None] == jnp.arange(total_experts, dtype=jnp.int32)[None, :]).astype(
        jnp.int32
    )
    earlier = jnp.sum((jnp.cumsum(onehot, axis=0) - onehot) * onehot, axis=1)
    return routed * capacity + earlier


def activation(gate_pre, up_pre, grad_scaled, weight_grid):
    sigmoid_val = jax.nn.sigmoid(gate_pre)
    silu_val = gate_pre * sigmoid_val
    hidden = silu_val * up_pre
    scaled = (weight_grid * hidden).astype(jnp.bfloat16)
    comb_part = jnp.sum(hidden * grad_scaled, axis=3)
    grad_hidden = weight_grid * grad_scaled
    grad_gate_pre = (
        grad_hidden * up_pre * sigmoid_val * (1.0 + gate_pre * (1.0 - sigmoid_val))
    ).astype(jnp.bfloat16)
    grad_up_pre = (grad_hidden * silu_val).astype(jnp.bfloat16)
    return (scaled, grad_gate_pre, grad_up_pre, comb_part)


def body(tokens, cotangent, experts, combine, w_gate, w_up, w_down):
    peers = lax.axis_size("ep")
    local_experts = w_gate.shape[0]
    total_experts = local_experts * peers
    tok_count = tokens.shape[0]
    picks = experts.shape[1]
    assigns = tok_count * picks
    capacity = 2 * assigns // total_experts
    per_peer = local_experts * capacity
    block_width = tokens.shape[1]
    slot_index = slot_positions(experts.reshape(assigns), total_experts, capacity)
    slot_owner = (
        jnp.zeros((total_experts * capacity,), jnp.int32)
        .at[slot_index]
        .set(jnp.arange(assigns, dtype=jnp.int32) + 1)
    )
    filled = slot_owner > 0
    source = jnp.maximum(slot_owner - 1, 0)
    token_ids = source // picks
    filled_col = filled[:, None]
    send_rows = jnp.where(
        filled_col, jnp.take(tokens, token_ids, axis=0), jnp.zeros((), jnp.bfloat16)
    ).reshape(peers, per_peer, block_width)
    send_cots = jnp.where(
        filled_col, jnp.take(cotangent, token_ids, axis=0), jnp.zeros((), jnp.bfloat16)
    ).reshape(peers, per_peer, block_width)
    send_weights = (
        jnp.where(filled, jnp.take(combine.reshape(assigns), source), jnp.float32(0.0))
        .astype(jnp.bfloat16)
        .reshape(peers, per_peer)
    )
    recv_rows, recv_cots, recv_weights = (
        lax.all_to_all(send_rows, "ep", split_axis=0, concat_axis=0, tiled=True),
        lax.all_to_all(send_cots, "ep", split_axis=0, concat_axis=0, tiled=True),
        lax.all_to_all(send_weights, "ep", split_axis=0, concat_axis=0, tiled=True),
    )
    rows_grid = recv_rows.reshape(peers, local_experts, capacity, block_width)
    cots_grid = recv_cots.reshape(peers, local_experts, capacity, block_width)
    weight_grid = recv_weights.astype(jnp.float32).reshape(peers, local_experts, capacity, 1)
    gate_part = jnp.einsum(
        "secd,edf->secf", rows_grid, w_gate, preferred_element_type=jnp.float32
    ).astype(jnp.bfloat16)
    up_part = jnp.einsum(
        "secd,edf->secf", rows_grid, w_up, preferred_element_type=jnp.float32
    ).astype(jnp.bfloat16)
    down_part = jnp.einsum(
        "secd,efd->secf", cots_grid, w_down, preferred_element_type=jnp.float32
    ).astype(jnp.bfloat16)
    gate_pre, up_pre, grad_scaled = (
        lax.psum(gate_part, "tp").astype(jnp.float32),
        lax.psum(up_part, "tp").astype(jnp.float32),
        lax.psum(down_part, "tp").astype(jnp.float32),
    )
    scaled, grad_gate_pre, grad_up_pre, comb_part = activation(
        gate_pre, up_pre, grad_scaled, weight_grid
    )
    down_grad = jnp.einsum("secf,secd->efd", scaled, cots_grid, preferred_element_type=jnp.float32)
    gate_grad = jnp.einsum(
        "secd,secf->edf", rows_grid, grad_gate_pre, preferred_element_type=jnp.float32
    )
    up_grad = jnp.einsum(
        "secd,secf->edf", rows_grid, grad_up_pre, preferred_element_type=jnp.float32
    )
    slot_sum = jnp.einsum(
        "secf,edf->secd", grad_gate_pre, w_gate, preferred_element_type=jnp.float32
    )
    slot_sum = slot_sum + jnp.einsum(
        "secf,edf->secd", grad_up_pre, w_up, preferred_element_type=jnp.float32
    )
    slot_grad = slot_sum.astype(jnp.bfloat16).reshape(peers, per_peer, block_width)
    returned = lax.all_to_all(slot_grad, "ep", split_axis=0, concat_axis=0, tiled=True)
    comb_back = lax.all_to_all(
        comb_part.reshape(peers, per_peer), "ep", split_axis=0, concat_axis=0, tiled=True
    )
    full_grad = returned.reshape(total_experts * capacity, block_width)
    per_assign = (
        jnp.take(full_grad, slot_index, axis=0)
        .astype(jnp.float32)
        .reshape(tok_count, picks, block_width)
    )
    grad_tokens = jnp.sum(per_assign, axis=1).astype(jnp.bfloat16)
    grad_combine = jnp.take(comb_back.reshape(total_experts * capacity), slot_index).reshape(
        tok_count, picks
    )
    return (grad_tokens, grad_combine, gate_grad, up_grad, down_grad)


MESH = pl.DeviceIdType.MESH
LANES = 128


def flip(index, mask, count):
    result, bit = 0, 1
    while bit < count:
        digit = lax.rem(lax.div(index, bit), 2)
        result = result + bit * ((1 - digit) if mask & bit else digit)
        bit *= 2
    return result


def dot(a, b, ca, cb):
    return lax.dot_general(a, b, (((ca,), (cb,)), ((), ())), preferred_element_type=jnp.float32)


def slot_table(first_expert, second_expert, base, slots, cap):
    count = first_expert.shape[1]
    row = lax.broadcasted_iota(jnp.int32, (slots, count), 0)
    expert = base + lax.shift_right_logical(row, cap.bit_length() - 1)
    number = jnp.bitwise_and(row, cap - 1).astype(jnp.float32)
    first = jnp.where(first_expert == expert, 1.0, 0.0)
    second = jnp.where(second_expert == expert, 1.0, 0.0)
    earlier = jnp.where(
        lax.broadcasted_iota(jnp.int32, (count, count), 0)
        < lax.broadcasted_iota(jnp.int32, (count, count), 1), 1.0, 0.0
    ).astype(jnp.bfloat16)
    position = dot((first + second).astype(jnp.bfloat16), earlier, 1, 0)
    here = jnp.where(position == number, 1.0, 0.0)
    return first * here, second * here


def fused_kernel(
    peers, parts, tokens_hbm, cotangent_hbm, experts_hbm, combine_hbm, gate_hbm, up_hbm, down_hbm,
    grad_tokens, grad_combine, gate_grad, up_grad, down_grad,
    tokens, cotangent, experts, combine, w_gate, w_up, w_down,
    send_t, send_c, cross_t, cross_c, cross_e, relay_t, relay_c, recv_t, recv_c,
    wsend, wrecv, part, core_in, pair, pair_in, acts, comb, slot, ret, ret_relay, out_relay, out_cross,
    comb_ret, gather, gather_relay, onehot_k,
    sem_in, sem_t, sem_c, sem_w, sem_e, sem_core, sem_pair, sem_act, sem_comb, sem_ret, sem_cret, sem_out,
):
    ep, tp = lax.axis_index("ep"), lax.axis_index("tp")
    core = lax.rem(tp, 2)
    mate = tp + 1 - 2 * core
    across = lax.rem(tp + 2, parts)
    width = tokens.shape[1]
    f = w_gate.shape[1]
    slots = recv_t.shape[0]
    cap = slots // peers
    half = peers // 2
    per_row = LANES // cap
    side_of, place = lax.div(ep, half), lax.rem(ep, half)
    peer = [flip(ep, d, peers) for d in range(peers)]
    spot = [lax.rem(p, half) for p in peer]

    def block(index, size=cap):
        return pl.ds(pl.multiple_of(index * size, size), size)

    def remote(src, dst, sems, index, device):
        return pltpu.make_async_remote_copy(
            src_ref=src, dst_ref=dst, send_sem=sems.at[0, index], recv_sem=sems.at[1, index],
            device_id=device, device_id_type=MESH,
        )

    loads = [
        pltpu.make_async_copy(source, target, sem_in.at[i])
        for i, (source, target) in enumerate((
            (experts_hbm, experts), (combine_hbm, combine), (tokens_hbm, tokens),
            (cotangent_hbm, cotangent), (gate_hbm.at[0], w_gate), (up_hbm.at[0], w_up),
            (down_hbm.at[0], w_down),
        ))
    ]
    for load in loads:
        load.start()
    barrier = pltpu.get_barrier_semaphore()
    for d in range(1, peers):
        pl.semaphore_signal(barrier, inc=1, device_id=(peer[d], tp), device_id_type=MESH)
    pl.semaphore_signal(barrier, inc=1, device_id=(ep, mate), device_id_type=MESH)
    pl.semaphore_signal(barrier, inc=1, device_id=(ep, across), device_id_type=MESH)
    loads[0].wait()
    loads[1].wait()

    first, second = slot_table(experts[0:1], experts[1:2], 0, slots, cap)
    onehot_k[0] = first
    onehot_k[1] = second
    gather[...] = (first + second).astype(jnp.bfloat16)
    weight = combine[...].astype(jnp.bfloat16).astype(jnp.float32)
    weight_column = jnp.sum(first * weight[0:1] + second * weight[1:2], axis=1, keepdims=True)
    for q in range(slots // LANES):
        wide = jnp.broadcast_to(weight_column[q * LANES:(q + 1) * LANES], (LANES, LANES))
        wsend[q] = wide.T[:8]
    wrecv[ep] = wsend[lax.div(ep, per_row)]
    loads[2].wait()
    loads[3].wait()
    pl.semaphore_wait(barrier, peers + 1)

    far = (peer[half], tp)
    send_e = remote(experts, cross_e, sem_e, 0, far)
    send_e.start()
    copy_t, copy_c, copy_w = {}, {}, {}
    own = gather[block(side_of, half * cap)]
    send_t[...] = dot(own, tokens[...], 1, 0).astype(jnp.bfloat16)
    send_c[...] = dot(own, cotangent[...], 1, 0).astype(jnp.bfloat16)
    for d in range(1, half):
        there = (peer[d], tp)
        copy_t[d] = remote(send_t.at[block(spot[d])], recv_t.at[block(ep)], sem_t, d, there)
        copy_t[d].start()
        copy_c[d] = remote(send_c.at[block(spot[d])], recv_c.at[block(ep)], sem_c, d, there)
        copy_c[d].start()
    copy_t[half] = remote(tokens, cross_t, sem_t, half, far)
    copy_t[half].start()
    copy_c[half] = remote(cotangent, cross_c, sem_c, half, far)
    copy_c[half].start()
    for d in range(1, peers):
        copy_w[d] = remote(
            wsend.at[lax.div(peer[d], per_row)], wrecv.at[ep], sem_w, d, (peer[d], tp)
        )
        copy_w[d].start()
    recv_t[block(ep)] = send_t[block(place)]
    recv_c[block(ep)] = send_c[block(place)]
    for load in loads[4:]:
        load.wait()

    def relay(kind, crossed, packed, landed, copies, sems):
        copies[half].wait_recv()
        packed[...] = dot(gather_relay[...], crossed[...], 1, 0).astype(jnp.bfloat16)
        for d in range(1, half):
            copies[half + d] = remote(
                packed.at[block(spot[d])], landed.at[block(peer[half])], sems, half + d, (peer[d], tp)
            )
            copies[half + d].start()
        landed[block(peer[half])] = packed[block(place)]

    pairs = peers // 2
    own_pair = lax.div(ep, 2)
    side = [flip(own_pair, j, pairs) for j in range(pairs)]
    core_copy, pair_copy, act_copy, comb_copy, ret_copy, cret_copy = {}, {}, {}, {}, {}, {}

    def stage_parts(j):
        for d in (2 * j, 2 * j + 1):
            if d:
                copy_w[d].wait_recv()
            if d not in (0, half):
                copy_t[d].wait_recv()
        rows = recv_t[block(side[j], 2 * cap)]
        part[j, :, :f] = dot(rows, w_gate[...], 1, 0).astype(jnp.bfloat16)
        part[j, :, f:2 * f] = dot(rows, w_up[...], 1, 0).astype(jnp.bfloat16)
        for d in (2 * j, 2 * j + 1):
            if d not in (0, half):
                copy_c[d].wait_recv()
        cots = recv_c[block(side[j], 2 * cap)]
        part[j, :, 2 * f:] = dot(cots, w_down[...], 1, 1).astype(jnp.bfloat16)
        core_copy[j] = remote(part.at[j, block(1 - core)], core_in.at[j], sem_core, j, (ep, mate))
        core_copy[j].start()

    def stage_pair(j):
        core_copy[j].wait_recv()
        mine = part[j, block(core)].astype(jnp.float32)
        pair[j] = (mine + core_in[j].astype(jnp.float32)).astype(jnp.bfloat16)
        pair_copy[j] = remote(pair.at[j], pair_in.at[j], sem_pair, j, (ep, across))
        pair_copy[j].start()

    def stage_act(j):
        pair_copy[j].wait_recv()
        source = 2 * side[j] + core
        gate_pre = pair[j, :, :f].astype(jnp.float32) + pair_in[j, :, :f].astype(jnp.float32)
        up_pre = pair[j, :, f:2 * f].astype(jnp.float32) + pair_in[j, :, f:2 * f].astype(jnp.float32)
        grad_scaled = pair[j, :, 2 * f:].astype(jnp.float32) + pair_in[j, :, 2 * f:].astype(jnp.float32)
        column = jnp.broadcast_to(wrecv[source][0:1], (LANES, LANES)).T
        w = column[:cap]
        for r in range(1, per_row):
            w = jnp.where(lax.rem(ep, per_row) == r, column[r * cap:(r + 1) * cap], w)
        w = w[:, 0:1]
        sigmoid = jax.nn.sigmoid(gate_pre)
        silu = gate_pre * sigmoid
        hidden = silu * up_pre
        grad_hidden = w * grad_scaled
        rows = block(source)
        acts[rows, :f] = (w * hidden).astype(jnp.bfloat16)
        acts[rows, f:2 * f] = (
            grad_hidden * up_pre * sigmoid * (1.0 + gate_pre * (1.0 - sigmoid))
        ).astype(jnp.bfloat16)
        acts[rows, 2 * f:] = (grad_hidden * silu).astype(jnp.bfloat16)
        act_copy[j] = remote(acts.at[rows], acts.at[rows], sem_act, j, (ep, mate))
        act_copy[j].start()
        total = jnp.sum(hidden * grad_scaled, axis=1, keepdims=True)
        wide = jnp.concatenate([jnp.broadcast_to(total, (cap, LANES))] * per_row, axis=0)
        comb[source] = wide.T[:8]
        comb_copy[j] = remote(comb.at[source], comb.at[source], sem_comb, j, (ep, mate))
        comb_copy[j].start()

    def stage_slot(j):
        act_copy[j].wait_recv()
        comb_copy[j].wait_recv()
        rows = block(side[j], 2 * cap)
        value = dot(acts[rows, f:2 * f], w_gate[...], 1, 1) + dot(acts[rows, 2 * f:], w_up[...], 1, 1)
        slot[rows] = value.astype(jnp.bfloat16)
        for d in (2 * j, 2 * j + 1):
            target = ret if d < half else ret_relay
            if d in (0, half):
                target[block(place)] = slot[block(peer[d])]
            else:
                ret_copy[d] = remote(
                    slot.at[block(peer[d])], target.at[block(place)], sem_ret, d, (peer[d % half], tp)
                )
                ret_copy[d].start()
            if d == 0:
                comb_ret[ep] = comb[ep]
            else:
                cret_copy[d] = remote(comb.at[peer[d]], comb_ret.at[ep], sem_cret, d, (peer[d], tp))
                cret_copy[d].start()

    near = range(pairs // 2)
    distant = range(pairs // 2, pairs)
    for j in near:
        stage_parts(j)
    for j in near:
        stage_pair(j)
    send_e.wait_recv()
    relay_first, relay_second = slot_table(
        cross_e[0:1], cross_e[1:2], side_of * half, half * cap, cap
    )
    gather_relay[...] = (relay_first + relay_second).astype(jnp.bfloat16)
    relay("t", cross_t, relay_t, recv_t, copy_t, sem_t)
    relay("c", cross_c, relay_c, recv_c, copy_c, sem_c)
    for j in near:
        stage_act(j)
    for j in near:
        stage_slot(j)
    for stage in (stage_parts, stage_pair, stage_act, stage_slot):
        for j in distant:
            stage(j)

    down_grad[...] = dot(acts[:, :f], recv_c[...], 0, 0)
    for d in range(half + 1, peers):
        ret_copy[d].wait_recv()
    out_relay[...] = dot(gather_relay[...], ret_relay[...], 0, 0).astype(jnp.bfloat16)
    send_out = remote(out_relay, out_cross, sem_out, 0, far)
    send_out.start()
    gate_grad[...] = dot(recv_t[...], acts[:, f:2 * f], 0, 0)
    up_grad[...] = dot(recv_t[...], acts[:, 2 * f:], 0, 0)

    for d in range(1, peers):
        cret_copy[d].wait_recv()
    part_lane = lax.broadcasted_iota(jnp.int32, (1, LANES), 1)
    totals = [jnp.zeros((1, tokens.shape[0]), jnp.float32)] * 2
    for q in range(slots // LANES):
        row = comb_ret[q * per_row][0:1]
        for r in range(1, per_row):
            row = jnp.where(part_lane >= r * cap, comb_ret[q * per_row + r][0:1], row)
        column = jnp.broadcast_to(row, (LANES, LANES)).T[:, 0:1]
        for k in range(2):
            chosen = onehot_k[k, q * LANES:(q + 1) * LANES] * column
            totals[k] = totals[k] + jnp.sum(chosen, axis=0, keepdims=True)
    for k in range(2):
        grad_combine[k:k + 1] = totals[k]
    for d in range(1, half):
        ret_copy[d].wait_recv()
    mine = dot(gather[block(side_of, half * cap)], ret[...], 0, 0)
    send_out.wait_recv()
    grad_tokens[...] = (mine + out_cross[...].astype(jnp.float32)).astype(jnp.bfloat16)
    send_e.wait_send()
    send_out.wait_send()
    for group in (
        copy_t, copy_c, copy_w, core_copy, pair_copy, act_copy, comb_copy, ret_copy, cret_copy
    ):
        for copy in group.values():
            copy.wait_send()


def store_kernel(count, *refs):
    sources, targets, sems = refs[:count], refs[count:2 * count], refs[2 * count]
    copies = [
        pltpu.make_async_copy(source, target, sems.at[i])
        for i, (source, target) in enumerate(zip(sources, targets))
    ]
    for copy in copies:
        copy.start()
    for copy in copies:
        copy.wait()


def fused_body(peers, parts, tokens, cotangent, experts, combine, w_gate, w_up, w_down):
    count, width = tokens.shape
    f = w_gate.shape[2]
    picks = experts.shape[1]
    cap = 2 * count * picks // peers
    slots = peers * cap
    pairs = peers // 2
    bf16, f32 = jnp.bfloat16, jnp.float32
    dma = pltpu.SemaphoreType.DMA
    vmem = pl.BlockSpec(memory_space=pltpu.VMEM)
    hbm = pl.BlockSpec(memory_space=pltpu.HBM)
    shapes = (
        jax.ShapeDtypeStruct((count, width), bf16),
        jax.ShapeDtypeStruct((picks, count), f32),
        jax.ShapeDtypeStruct((width, f), f32),
        jax.ShapeDtypeStruct((width, f), f32),
        jax.ShapeDtypeStruct((f, width), f32),
    )
    half_rows = pltpu.VMEM((slots // 2, width), bf16)
    rows = pltpu.VMEM((count, width), bf16)
    landed = pltpu.VMEM((slots, width), bf16)
    sums = pltpu.VMEM((pairs, cap, 3 * f), bf16)
    small = pltpu.VMEM((peers, 8, LANES), f32)
    outs = pl.pallas_call(
        functools.partial(fused_kernel, peers, parts),
        out_shape=shapes,
        in_specs=[hbm] * 7,
        out_specs=(vmem,) * 5,
        scratch_shapes=[
            rows, rows, pltpu.VMEM((picks, count), jnp.int32), pltpu.VMEM((picks, count), f32),
            pltpu.VMEM((width, f), bf16), pltpu.VMEM((width, f), bf16), pltpu.VMEM((f, width), bf16),
            half_rows, half_rows, rows, rows, pltpu.VMEM((picks, count), jnp.int32),
            half_rows, half_rows, landed, landed,
            pltpu.VMEM((slots // LANES, 8, LANES), f32), small,
            pltpu.VMEM((pairs, 2 * cap, 3 * f), bf16), sums, sums, sums,
            pltpu.VMEM((slots, 3 * f), bf16), small, landed, half_rows, half_rows, rows, rows,
            small, pltpu.VMEM((slots, count), bf16), pltpu.VMEM((slots // 2, count), bf16),
            pltpu.VMEM((picks, slots, count), f32),
            dma((7,)), dma((2, peers)), dma((2, peers)), dma((2, peers)), dma((2, 1)),
            dma((2, pairs)), dma((2, pairs)), dma((2, pairs)), dma((2, pairs)),
            dma((2, peers)), dma((2, peers)), dma((2, 1)),
        ],
        compiler_params=pltpu.CompilerParams(
            collective_id=0, has_side_effects=True, vmem_limit_bytes=48 * 1024 * 1024
        ),
    )(*(
        pltpu.with_memory_space_constraint(x, pltpu.HBM)
        for x in (tokens, cotangent, experts.T, combine.T, w_gate, w_up, w_down)
    ))
    outs = pl.pallas_call(
        functools.partial(store_kernel, len(outs)),
        out_shape=shapes,
        in_specs=[vmem] * 5,
        out_specs=(hbm,) * 5,
        scratch_shapes=[dma((5,))],
        compiler_params=pltpu.CompilerParams(vmem_limit_bytes=1024 * 1024),
    )(*outs)
    return outs[0], outs[1].T, outs[2][None], outs[3][None], outs[4][None]


def choose(mesh, tokens, cotangent, experts, combine, w_gate, w_up, w_down):
    peers, parts = mesh.shape["ep"], mesh.shape["tp"]
    count, width = tokens.shape
    cap = 2 * count * experts.shape[1] // w_gate.shape[0] // peers
    fits = (
        w_gate.shape[0] == 1 and experts.shape[1] == 2 and parts == 4
        and peers in (4, 8, 16) and cap in (16, 32, 64, 128)
        and count % LANES == 0 and width % LANES == 0
        and w_gate.shape[2] % LANES == 0 and peers * cap % LANES == 0
    )
    run = functools.partial(fused_body, peers, parts) if fits else body
    return run(tokens, cotangent, experts, combine, w_gate, w_up, w_down)


def solution(mesh):
    return jax.shard_map(
        functools.partial(choose, mesh),
        mesh=mesh,
        in_specs=(
            P("ep", "tp"),
            P("ep", "tp"),
            P("ep", None),
            P("ep", None),
            P("ep", "tp", None),
            P("ep", "tp", None),
            P("ep", None, "tp"),
        ),
        out_specs=(
            P("ep", "tp"),
            P("ep", None),
            P("ep", "tp", None),
            P("ep", "tp", None),
            P("ep", None, "tp"),
        ),
        check_vma=False,
    )
```

profile of v0, /device:TPU:0, one launch (start us, length us, event | category | flops | bytes accessed | tf_op | source)
XLA Modules:
  0.0 53.7 jit_solution(3966507865391959459)
XLA Ops:
  0.6 51.8 %shard_map.110 = (bf16[128,512]{1,0:T(8,128)(2,1)S(1)}, f32[2,128]{1,0:T(2,128)S(1)}, f32[512,256]{1,0:T(8,128)S(1)}, f32[512,256]{1,0:T(8,128)S(1)}, f32[256,512]{1,0:T(8,128)S(1)}) custom-call(bf16[128,512]{1,0:T(8,128)(2,1)} %tokens_hbm.1, bf16[128,512]{1,0:T(8,128)(2,1)} %cotangent_hbm.1, s32[2,128]{1,0:T(2,128)} %bitcast.6, f32[2,128]{1,0:T(2,128)} %bitcast.7, ...), custom_call_target="tpu_custom_call" | custom-call | tf_op jit(solution)/shard_map/pallas_call | solution.py:426
  52.5 1.2 %shard_map.111 = (bf16[128,512]{1,0:T(8,128)(2,1)}, f32[2,128]{1,0:T(2,128)}, f32[512,256]{1,0:T(8,128)}, f32[512,256]{1,0:T(8,128)}, f32[256,512]{1,0:T(8,128)}) custom-call(bf16[128,512]{1,0:T(8,128)(2,1)S(1)} %get-tuple-element.15.refs_0_, f32[2,128]{1,0:T(2,128)S(1)} %get-tuple-element.16.refs_1_, f32[512,256]{1,0:T(8,128)S(1)} %get-tuple-element.17.refs_2_, ...), custom_call_target="tpu_custom_call" | custom-call | tf_op jit(solution)/shard_map/pallas_call | solution.py:452
where the time goes:
time: 53.9 us; the launch traced here: 53.7 us
  Pallas kernels  53.1 us (99%)
  between operations  0.64 us (1%)
    pallas_call x1, Pallas kernels, fused_body(): pl.pallas_call(functools.partial(fused_kernel, peers, parts), out_shape=s...  51.8 us
    pallas_call x1, Pallas kernels, fused_body(): pl.pallas_call(functools.partial(store_kernel, len(outs)), out_shape=shap...  1.23 us

commit v1 on v0

--- a/solution.py
+++ b/solution.py
@@ -155,15 +155,16 @@
     grad_tokens, grad_combine, gate_grad, up_grad, down_grad,
     tokens, cotangent, experts, combine, w_gate, w_up, w_down,
     send_t, send_c, cross_t, cross_c, cross_e, relay_t, relay_c, recv_t, recv_c,
-    wsend, wrecv, part, core_in, pair, pair_in, acts, comb, slot, ret, ret_relay, out_relay, out_cross,
+    wsend, wrecv, part_t, part_c, core_t, core_c, pair_t, pair_c, pair_in_t, pair_in_c,
+    acts, comb, slot, ret,
     comb_ret, gather, gather_relay, onehot_k,
-    sem_in, sem_t, sem_c, sem_w, sem_e, sem_core, sem_pair, sem_act, sem_comb, sem_ret, sem_cret, sem_out,
+    sem_in, sem_t, sem_c, sem_rt, sem_rc, sem_xt, sem_xc, sem_w, sem_e,
+    sem_core, sem_pair, sem_act, sem_comb, sem_ret, sem_cret,
 ):
     ep, tp = lax.axis_index("ep"), lax.axis_index("tp")
     core = lax.rem(tp, 2)
     mate = tp + 1 - 2 * core
     across = lax.rem(tp + 2, parts)
-    width = tokens.shape[1]
     f = w_gate.shape[1]
     slots = recv_t.shape[0]
     cap = slots // peers
@@ -172,6 +173,11 @@
     side_of, place = lax.div(ep, half), lax.rem(ep, half)
     peer = [flip(ep, d, peers) for d in range(peers)]
     spot = [lax.rem(p, half) for p in peer]
+    layer, column = lax.div(ep, 2), lax.rem(ep, 2)
+    inner = jnp.where(layer == 1 + side_of, 1, 0)
+    is_inner, is_outer = inner == 1, inner == 0
+    layers = (layer, layer + 1 - 2 * lax.rem(layer, 2), 2 - side_of, 3 * (1 - side_of))
+    far_gate = (2 * layers[2] + column, tp)
 
     def block(index, size=cap):
         return pl.ds(pl.multiple_of(index * size, size), size)
@@ -212,84 +218,145 @@
     wrecv[ep] = wsend[lax.div(ep, per_row)]
     loads[2].wait()
     loads[3].wait()
-    pl.semaphore_wait(barrier, peers + 1)
-
-    far = (peer[half], tp)
-    send_e = remote(experts, cross_e, sem_e, 0, far)
+    with jax.named_scope("barrier"):
+        pl.semaphore_wait(barrier, peers + 1)
+
+    own = gather[block(side_of, half * cap)]
+    send_e = remote(experts, cross_e.at[1 - inner], sem_e, 1 - inner, far_gate)
     send_e.start()
-    copy_t, copy_c, copy_w = {}, {}, {}
-    own = gather[block(side_of, half * cap)]
-    send_t[...] = dot(own, tokens[...], 1, 0).astype(jnp.bfloat16)
-    send_c[...] = dot(own, cotangent[...], 1, 0).astype(jnp.bfloat16)
-    for d in range(1, half):
-        there = (peer[d], tp)
-        copy_t[d] = remote(send_t.at[block(spot[d])], recv_t.at[block(ep)], sem_t, d, there)
-        copy_t[d].start()
-        copy_c[d] = remote(send_c.at[block(spot[d])], recv_c.at[block(ep)], sem_c, d, there)
-        copy_c[d].start()
-    copy_t[half] = remote(tokens, cross_t, sem_t, half, far)
-    copy_t[half].start()
-    copy_c[half] = remote(cotangent, cross_c, sem_c, half, far)
-    copy_c[half].start()
+    copy_w = {}
     for d in range(1, peers):
         copy_w[d] = remote(
             wsend.at[lax.div(peer[d], per_row)], wrecv.at[ep], sem_w, d, (peer[d], tp)
         )
         copy_w[d].start()
-    recv_t[block(ep)] = send_t[block(place)]
-    recv_c[block(ep)] = send_c[block(place)]
+    raw_t = remote(tokens, cross_t.at[1 - inner], sem_xt, 1 - inner, far_gate)
+    raw_c = remote(cotangent, cross_c.at[1 - inner], sem_xc, 1 - inner, far_gate)
+
+    raw_t.start()
+    raw_c.start()
+
+    def near_copy(d, packed, landed, sems):
+        return remote(packed.at[block(spot[d])], landed.at[block(ep)], sems, d, (peer[d], tp))
+
+    for source, packed, landed, sems in (
+        (tokens, send_t, recv_t, sem_t), (cotangent, send_c, recv_c, sem_c)
+    ):
+        packed[...] = dot(own, source[...], 1, 0).astype(jnp.bfloat16)
+        for d in (1, 2, 3):
+            near_copy(d, packed, landed, sems).start()
+        landed[block(ep)] = packed[block(place)]
+
     for load in loads[4:]:
         load.wait()
 
-    def relay(kind, crossed, packed, landed, copies, sems):
-        copies[half].wait_recv()
-        packed[...] = dot(gather_relay[...], crossed[...], 1, 0).astype(jnp.bfloat16)
-        for d in range(1, half):
-            copies[half + d] = remote(
-                packed.at[block(spot[d])], landed.at[block(peer[half])], sems, half + d, (peer[d], tp)
-            )
-            copies[half + d].start()
-        landed[block(peer[half])] = packed[block(place)]
+    def relay_copy(k, d, packed, landed, sems):
+        return remote(
+            packed.at[k, block(spot[d])], landed.at[block(2 * layers[2 + k] + column)],
+            sems, 4 * k + d, (peer[d], tp),
+        )
+
+    def relay_table(k):
+        remote(experts, cross_e.at[k], sem_e, k, far_gate).wait_recv()
+        chosen_a, chosen_b = slot_table(
+            cross_e[k, 0:1], cross_e[k, 1:2], side_of * half, half * cap, cap
+        )
+        gather_relay[k] = (chosen_a + chosen_b).astype(jnp.bfloat16)
+
+    def relay(k, source, crossed, packed, landed, sems_in, sems_out):
+        with jax.named_scope("wait_raw"):
+            remote(source, crossed.at[k], sems_in, k, far_gate).wait_recv()
+        packed[k] = dot(gather_relay[k], crossed[k], 1, 0).astype(jnp.bfloat16)
+        for d in (2, 3, 1):
+            relay_copy(k, d, packed, landed, sems_out).start()
+        landed[block(2 * layers[2 + k] + column)] = packed[k, block(place)]
+
+    def relay_tokens(k, gate):
+        relay(k, tokens, cross_t, relay_t, recv_t, sem_xt, sem_rt)
+
+    def relay_cots(k, gate):
+        relay(k, cotangent, cross_c, relay_c, recv_c, sem_xc, sem_rc)
+
+    def arrive(j, gate, packed, relayed, landed, near_sems, sems):
+        if j < 2:
+            for d in (2 * j, 2 * j + 1):
+                if d:
+                    near_copy(d, packed, landed, near_sems).wait_recv()
+        else:
+            for d in (1,) if gate else (2, 3):
+                with jax.named_scope("arrive%d" % d):
+                    relay_copy(j - 2, d, relayed, landed, sems).wait_recv()
 
     pairs = peers // 2
-    own_pair = lax.div(ep, 2)
-    side = [flip(own_pair, j, pairs) for j in range(pairs)]
-    core_copy, pair_copy, act_copy, comb_copy, ret_copy, cret_copy = {}, {}, {}, {}, {}, {}
-
-    def stage_parts(j):
-        for d in (2 * j, 2 * j + 1):
-            if d:
+
+    def core_copy(i):
+        part, landed = (part_t, core_t) if i < pairs else (part_c, core_c)
+        j = i % pairs
+        return remote(part.at[j, block(1 - core)], landed.at[j], sem_core, i, (ep, mate))
+
+    def pair_copy(i):
+        summed, landed = (pair_t, pair_in_t) if i < pairs else (pair_c, pair_in_c)
+        return remote(summed.at[i % pairs], landed.at[i % pairs], sem_pair, i, (ep, across))
+
+    def act_copy(j):
+        rows = block(2 * layers[j] + core)
+        return remote(acts.at[rows], acts.at[rows], sem_act, j, (ep, mate))
+
+    def comb_copy(j):
+        source = 2 * layers[j] + core
+        return remote(comb.at[source], comb.at[source], sem_comb, j, (ep, mate))
+
+    def distance(j, b):
+        return 2 * j + b if j < 2 else 4 + 2 * lax.rem(j + inner, 2) + b
+
+    def back_copies(j, b):
+        target = 2 * layers[j] + lax.rem(column + b, 2)
+        return (
+            remote(
+                slot.at[block(target)], ret.at[block(ep)], sem_ret, distance(j, b), (target, tp)
+            ),
+            remote(comb.at[target], comb_ret.at[ep], sem_cret, distance(j, b), (target, tp)),
+        )
+
+    def parts_tokens(j, gate):
+        arrive(j, gate, send_t, relay_t, recv_t, sem_t, sem_rt)
+        rows = recv_t[block(layers[j], 2 * cap)]
+        part_t[j, :, :f] = dot(rows, w_gate[...], 1, 0).astype(jnp.bfloat16)
+        part_t[j, :, f:] = dot(rows, w_up[...], 1, 0).astype(jnp.bfloat16)
+        core_copy(j).start()
+
+    def parts_cots(j, gate):
+        arrive(j, gate, send_c, relay_c, recv_c, sem_c, sem_rc)
+        cots = recv_c[block(layers[j], 2 * cap)]
+        part_c[j] = dot(cots, w_down[...], 1, 1).astype(jnp.bfloat16)
+        core_copy(pairs + j).start()
+
+    def pair_sum(j, i, part, landed, summed):
+        core_copy(i).wait_recv()
+        mine = part[j, block(core)].astype(jnp.float32)
+        summed[j] = (mine + landed[j].astype(jnp.float32)).astype(jnp.bfloat16)
+        pair_copy(i).start()
+
+    def pair_tokens(j, gate):
+        pair_sum(j, j, part_t, core_t, pair_t)
+
+    def pair_cots(j, gate):
+        pair_sum(j, pairs + j, part_c, core_c, pair_c)
+
+    def act(j, gate):
+        if j == 0:
+            for d in range(1, peers):
                 copy_w[d].wait_recv()
-            if d not in (0, half):
-                copy_t[d].wait_recv()
-        rows = recv_t[block(side[j], 2 * cap)]
-        part[j, :, :f] = dot(rows, w_gate[...], 1, 0).astype(jnp.bfloat16)
-        part[j, :, f:2 * f] = dot(rows, w_up[...], 1, 0).astype(jnp.bfloat16)
-        for d in (2 * j, 2 * j + 1):
-            if d not in (0, half):
-                copy_c[d].wait_recv()
-        cots = recv_c[block(side[j], 2 * cap)]
-        part[j, :, 2 * f:] = dot(cots, w_down[...], 1, 1).astype(jnp.bfloat16)
-        core_copy[j] = remote(part.at[j, block(1 - core)], core_in.at[j], sem_core, j, (ep, mate))
-        core_copy[j].start()
-
-    def stage_pair(j):
-        core_copy[j].wait_recv()
-        mine = part[j, block(core)].astype(jnp.float32)
-        pair[j] = (mine + core_in[j].astype(jnp.float32)).astype(jnp.bfloat16)
-        pair_copy[j] = remote(pair.at[j], pair_in.at[j], sem_pair, j, (ep, across))
-        pair_copy[j].start()
-
-    def stage_act(j):
-        pair_copy[j].wait_recv()
-        source = 2 * side[j] + core
-        gate_pre = pair[j, :, :f].astype(jnp.float32) + pair_in[j, :, :f].astype(jnp.float32)
-        up_pre = pair[j, :, f:2 * f].astype(jnp.float32) + pair_in[j, :, f:2 * f].astype(jnp.float32)
-        grad_scaled = pair[j, :, 2 * f:].astype(jnp.float32) + pair_in[j, :, 2 * f:].astype(jnp.float32)
-        column = jnp.broadcast_to(wrecv[source][0:1], (LANES, LANES)).T
-        w = column[:cap]
+        pair_copy(j).wait_recv()
+        pair_copy(pairs + j).wait_recv()
+        source = 2 * layers[j] + core
+        gate_pre = pair_t[j, :, :f].astype(jnp.float32) + pair_in_t[j, :, :f].astype(jnp.float32)
+        up_pre = pair_t[j, :, f:].astype(jnp.float32) + pair_in_t[j, :, f:].astype(jnp.float32)
+        grad_scaled = pair_c[j].astype(jnp.float32) + pair_in_c[j].astype(jnp.float32)
+        weights = jnp.broadcast_to(wrecv[source][0:1], (LANES, LANES)).T
+        w = weights[:cap]
         for r in range(1, per_row):
-            w = jnp.where(lax.rem(ep, per_row) == r, column[r * cap:(r + 1) * cap], w)
+            w = jnp.where(lax.rem(ep, per_row) == r, weights[r * cap:(r + 1) * cap], w)
         w = w[:, 0:1]
         sigmoid = jax.nn.sigmoid(gate_pre)
         silu = gate_pre * sigmoid
@@ -301,91 +368,102 @@
             grad_hidden * up_pre * sigmoid * (1.0 + gate_pre * (1.0 - sigmoid))
         ).astype(jnp.bfloat16)
         acts[rows, 2 * f:] = (grad_hidden * silu).astype(jnp.bfloat16)
-        act_copy[j] = remote(acts.at[rows], acts.at[rows], sem_act, j, (ep, mate))
-        act_copy[j].start()
+        act_copy(j).start()
         total = jnp.sum(hidden * grad_scaled, axis=1, keepdims=True)
         wide = jnp.concatenate([jnp.broadcast_to(total, (cap, LANES))] * per_row, axis=0)
         comb[source] = wide.T[:8]
-        comb_copy[j] = remote(comb.at[source], comb.at[source], sem_comb, j, (ep, mate))
-        comb_copy[j].start()
-
-    def stage_slot(j):
-        act_copy[j].wait_recv()
-        comb_copy[j].wait_recv()
-        rows = block(side[j], 2 * cap)
+        comb_copy(j).start()
+
+    def slots_back(j, gate):
+        act_copy(j).wait_recv()
+        comb_copy(j).wait_recv()
+        rows = block(layers[j], 2 * cap)
         value = dot(acts[rows, f:2 * f], w_gate[...], 1, 1) + dot(acts[rows, 2 * f:], w_up[...], 1, 1)
         slot[rows] = value.astype(jnp.bfloat16)
-        for d in (2 * j, 2 * j + 1):
-            target = ret if d < half else ret_relay
-            if d in (0, half):
-                target[block(place)] = slot[block(peer[d])]
-            else:
-                ret_copy[d] = remote(
-                    slot.at[block(peer[d])], target.at[block(place)], sem_ret, d, (peer[d % half], tp)
-                )
-                ret_copy[d].start()
-            if d == 0:
+        for b in range(2):
+            if j == b == 0:
+                ret[block(ep)] = slot[block(ep)]
                 comb_ret[ep] = comb[ep]
             else:
-                cret_copy[d] = remote(comb.at[peer[d]], comb_ret.at[ep], sem_cret, d, (peer[d], tp))
-                cret_copy[d].start()
-
-    near = range(pairs // 2)
-    distant = range(pairs // 2, pairs)
-    for j in near:
-        stage_parts(j)
-    for j in near:
-        stage_pair(j)
-    send_e.wait_recv()
-    relay_first, relay_second = slot_table(
-        cross_e[0:1], cross_e[1:2], side_of * half, half * cap, cap
-    )
-    gather_relay[...] = (relay_first + relay_second).astype(jnp.bfloat16)
-    relay("t", cross_t, relay_t, recv_t, copy_t, sem_t)
-    relay("c", cross_c, relay_c, recv_c, copy_c, sem_c)
-    for j in near:
-        stage_act(j)
-    for j in near:
-        stage_slot(j)
-    for stage in (stage_parts, stage_pair, stage_act, stage_slot):
-        for j in distant:
-            stage(j)
-
-    down_grad[...] = dot(acts[:, :f], recv_c[...], 0, 0)
-    for d in range(half + 1, peers):
-        ret_copy[d].wait_recv()
-    out_relay[...] = dot(gather_relay[...], ret_relay[...], 0, 0).astype(jnp.bfloat16)
-    send_out = remote(out_relay, out_cross, sem_out, 0, far)
-    send_out.start()
-    gate_grad[...] = dot(recv_t[...], acts[:, f:2 * f], 0, 0)
-    up_grad[...] = dot(recv_t[...], acts[:, 2 * f:], 0, 0)
-
-    for d in range(1, peers):
-        cret_copy[d].wait_recv()
+                for copy in back_copies(j, b):
+                    copy.start()
+
+    def tables(k, gate):
+        relay_table(k)
+
+    def grads(which, gate):
+        if which == 0:
+            down_grad[...] = dot(acts[:, :f], recv_c[...], 0, 0)
+        elif which == 1:
+            gate_grad[...] = dot(recv_t[...], acts[:, f:2 * f], 0, 0)
+        else:
+            up_grad[...] = dot(recv_t[...], acts[:, 2 * f:], 0, 0)
+
+    names = {
+        "T": tables, "rt": relay_tokens, "rc": relay_cots, "pt": parts_tokens, "pc": parts_cots,
+        "st": pair_tokens, "sc": pair_cots, "a": act, "b": slots_back, "g": grads,
+    }
+    outer_order = (
+        "pt0", "pc0", "st0", "sc0", "pt1", "st1", "pc1", "sc1", "a0", "b0", "pt3", "st3",
+        "a1", "b1", "pc3", "sc3", "pt2", "st2", "a3", "b3", "pc2", "sc2", "a2", "b2",
+    )
+    inner_order = (
+        "pt0", "T1", "pc0", "st0", "T0", "sc0", "rt1", "a0", "rc1", "b0", "pt3", "st3",
+        "rt0", "pt1", "st1", "pc3", "sc3", "rc0", "pc1", "sc1", "a3", "pt2", "st2", "a1",
+        "b3", "b1", "pc2", "sc2", "a2", "b2",
+    )
+    for role, order, gate in ((is_outer, outer_order, False), (is_inner, inner_order, True)):
+        @pl.when(role)
+        def _():
+            for word in order:
+                with jax.named_scope(word):
+                    names[word[:-1]](int(word[-1]), gate)
+
+    for which in range(3):
+        with jax.named_scope("g%d" % which):
+            grads(which, None)
+
+    with jax.named_scope("cret"):
+        for d in range(1, peers):
+            remote(comb.at[0], comb_ret.at[0], sem_cret, d, (peer[d], tp)).wait_recv()
     part_lane = lax.broadcasted_iota(jnp.int32, (1, LANES), 1)
     totals = [jnp.zeros((1, tokens.shape[0]), jnp.float32)] * 2
     for q in range(slots // LANES):
         row = comb_ret[q * per_row][0:1]
         for r in range(1, per_row):
             row = jnp.where(part_lane >= r * cap, comb_ret[q * per_row + r][0:1], row)
-        column = jnp.broadcast_to(row, (LANES, LANES)).T[:, 0:1]
+        values = jnp.broadcast_to(row, (LANES, LANES)).T[:, 0:1]
         for k in range(2):
-            chosen = onehot_k[k, q * LANES:(q + 1) * LANES] * column
+            chosen = onehot_k[k, q * LANES:(q + 1) * LANES] * values
             totals[k] = totals[k] + jnp.sum(chosen, axis=0, keepdims=True)
     for k in range(2):
         grad_combine[k:k + 1] = totals[k]
+    with jax.named_scope("ret"):
+        for d in range(1, peers):
+            remote(slot.at[block(0)], ret.at[block(0)], sem_ret, d, (peer[d], tp)).wait_recv()
+    grad_tokens[...] = dot(gather[...], ret[...], 0, 0).astype(jnp.bfloat16)
+    for copy in (send_e, raw_t, raw_c, *copy_w.values()):
+        copy.wait_send()
     for d in range(1, half):
-        ret_copy[d].wait_recv()
-    mine = dot(gather[block(side_of, half * cap)], ret[...], 0, 0)
-    send_out.wait_recv()
-    grad_tokens[...] = (mine + out_cross[...].astype(jnp.float32)).astype(jnp.bfloat16)
-    send_e.wait_send()
-    send_out.wait_send()
-    for group in (
-        copy_t, copy_c, copy_w, core_copy, pair_copy, act_copy, comb_copy, ret_copy, cret_copy
-    ):
-        for copy in group.values():
+        near_copy(d, send_t, recv_t, sem_t).wait_send()
+        near_copy(d, send_c, recv_c, sem_c).wait_send()
+    for j in range(pairs):
+        for copy in (
+            core_copy(j), core_copy(pairs + j), pair_copy(j), pair_copy(pairs + j),
+            act_copy(j), comb_copy(j),
+        ):
             copy.wait_send()
+        for b in range(2):
+            if j or b:
+                for copy in back_copies(j, b):
+                    copy.wait_send()
+
+    @pl.when(is_inner)
+    def _():
+        for k in range(2):
+            for d in range(1, half):
+                relay_copy(k, d, relay_t, recv_t, sem_rt).wait_send()
+                relay_copy(k, d, relay_c, recv_c, sem_rc).wait_send()
 
 
 def store_kernel(count, *refs):
@@ -419,9 +497,12 @@
         jax.ShapeDtypeStruct((f, width), f32),
     )
     half_rows = pltpu.VMEM((slots // 2, width), bf16)
+    relayed = pltpu.VMEM((2, slots // 2, width), bf16)
     rows = pltpu.VMEM((count, width), bf16)
+    crossed = pltpu.VMEM((2, count, width), bf16)
     landed = pltpu.VMEM((slots, width), bf16)
-    sums = pltpu.VMEM((pairs, cap, 3 * f), bf16)
+    sums_t = pltpu.VMEM((pairs, cap, 2 * f), bf16)
+    sums_c = pltpu.VMEM((pairs, cap, f), bf16)
     small = pltpu.VMEM((peers, 8, LANES), f32)
     outs = pl.pallas_call(
         functools.partial(fused_kernel, peers, parts),
@@ -431,16 +512,18 @@
         scratch_shapes=[
             rows, rows, pltpu.VMEM((picks, count), jnp.int32), pltpu.VMEM((picks, count), f32),
             pltpu.VMEM((width, f), bf16), pltpu.VMEM((width, f), bf16), pltpu.VMEM((f, width), bf16),
-            half_rows, half_rows, rows, rows, pltpu.VMEM((picks, count), jnp.int32),
-            half_rows, half_rows, landed, landed,
+            half_rows, half_rows, crossed, crossed, pltpu.VMEM((2, picks, count), jnp.int32),
+            relayed, relayed, landed, landed,
             pltpu.VMEM((slots // LANES, 8, LANES), f32), small,
-            pltpu.VMEM((pairs, 2 * cap, 3 * f), bf16), sums, sums, sums,
-            pltpu.VMEM((slots, 3 * f), bf16), small, landed, half_rows, half_rows, rows, rows,
-            small, pltpu.VMEM((slots, count), bf16), pltpu.VMEM((slots // 2, count), bf16),
+            pltpu.VMEM((pairs, 2 * cap, 2 * f), bf16), pltpu.VMEM((pairs, 2 * cap, f), bf16),
+            sums_t, sums_c, sums_t, sums_c, sums_t, sums_c,
+            pltpu.VMEM((slots, 3 * f), bf16), small, landed, landed,
+            small, pltpu.VMEM((slots, count), bf16), pltpu.VMEM((2, slots // 2, count), bf16),
             pltpu.VMEM((picks, slots, count), f32),
-            dma((7,)), dma((2, peers)), dma((2, peers)), dma((2, peers)), dma((2, 1)),
-            dma((2, pairs)), dma((2, pairs)), dma((2, pairs)), dma((2, pairs)),
-            dma((2, peers)), dma((2, peers)), dma((2, 1)),
+            dma((7,)), dma((2, peers)), dma((2, peers)), dma((2, peers)), dma((2, peers)),
+            dma((2, 2)), dma((2, 2)), dma((2, peers)), dma((2, 2)),
+            dma((2, 2 * pairs)), dma((2, 2 * pairs)), dma((2, pairs)), dma((2, pairs)),
+            dma((2, peers)), dma((2, peers)),
         ],
         compiler_params=pltpu.CompilerParams(
             collective_id=0, has_side_effects=True, vmem_limit_bytes=48 * 1024 * 1024
@@ -466,7 +549,7 @@
     cap = 2 * count * experts.shape[1] // w_gate.shape[0] // peers
     fits = (
         w_gate.shape[0] == 1 and experts.shape[1] == 2 and parts == 4
-        and peers in (4, 8, 16) and cap in (16, 32, 64, 128)
+        and peers == 8 and cap in (16, 32, 64, 128)
         and count % LANES == 0 and width % LANES == 0
         and w_gate.shape[2] % LANES == 0 and peers * cap % LANES == 0
     )

time: 53.9 us -> 43.4 us (0.81)
  the two profiles are of different devices: /device:TPU:0 before, /device:TPU:18 now
where the time goes in v1:
time: 43.4 us; the launch traced here: 42.5 us
  Pallas kernels  41.9 us (97%)
  between operations  0.64 us (1%)
    pallas_call x1, Pallas kernels, fused_body(): pl.pallas_call(functools.partial(fused_kernel, peers, parts), out_shape=s...  40.7 us
    pallas_call x1, Pallas kernels, fused_body(): pl.pallas_call(functools.partial(store_kernel, len(outs)), out_shape=shap...  1.23 us

profile of v1, /device:TPU:18, one launch (start us, length us, event | category | flops | bytes accessed | tf_op | source)
XLA Modules:
  0.0 42.5 jit_solution(432122997234938374)
XLA Ops:
  0.6 40.7 %shard_map.110 = (bf16[128,512]{1,0:T(8,128)(2,1)S(1)}, f32[2,128]{1,0:T(2,128)S(1)}, f32[512,256]{1,0:T(8,128)S(1)}, f32[512,256]{1,0:T(8,128)S(1)}, f32[256,512]{1,0:T(8,128)S(1)}) custom-call(bf16[128,512]{1,0:T(8,128)(2,1)} %tokens_hbm.1, bf16[128,512]{1,0:T(8,128)(2,1)} %cotangent_hbm.1, s32[2,128]{1,0:T(2,128)} %bitcast.6, f32[2,128]{1,0:T(2,128)} %bitcast.7, ...), custom_call_target="tpu_custom_call" | custom-call | tf_op jit(solution)/shard_map/pallas_call | solution.py:507
  41.3 1.2 %shard_map.111 = (bf16[128,512]{1,0:T(8,128)(2,1)}, f32[2,128]{1,0:T(2,128)}, f32[512,256]{1,0:T(8,128)}, f32[512,256]{1,0:T(8,128)}, f32[256,512]{1,0:T(8,128)}) custom-call(bf16[128,512]{1,0:T(8,128)(2,1)S(1)} %get-tuple-element.15.refs_0_, f32[2,128]{1,0:T(2,128)S(1)} %get-tuple-element.16.refs_1_, f32[512,256]{1,0:T(8,128)S(1)} %get-tuple-element.17.refs_2_, ...), custom_call_target="tpu_custom_call" | custom-call | tf_op jit(solution)/shard_map/pallas_call | solution.py:535

commit v2 on v1

--- a/solution.py
+++ b/solution.py
@@ -158,8 +158,8 @@
     wsend, wrecv, part_t, part_c, core_t, core_c, pair_t, pair_c, pair_in_t, pair_in_c,
     acts, comb, slot, ret,
     comb_ret, gather, gather_relay, onehot_k,
-    sem_in, sem_t, sem_c, sem_rt, sem_rc, sem_xt, sem_xc, sem_w, sem_e,
-    sem_core, sem_pair, sem_act, sem_comb, sem_ret, sem_cret,
+    sem_in, sem_t, sem_c, sem_rt, sem_rc, sem_x, sem_w, sem_e,
+    sem_core, sem_pair, sem_act, sem_ret, sem_cret,
 ):
     ep, tp = lax.axis_index("ep"), lax.axis_index("tp")
     core = lax.rem(tp, 2)
@@ -182,11 +182,17 @@
     def block(index, size=cap):
         return pl.ds(pl.multiple_of(index * size, size), size)
 
-    def remote(src, dst, sems, index, device):
+    def remote(src, dst, sems, sent, landed, device):
         return pltpu.make_async_remote_copy(
-            src_ref=src, dst_ref=dst, send_sem=sems.at[0, index], recv_sem=sems.at[1, index],
+            src_ref=src, dst_ref=dst, send_sem=sems.at[sent], recv_sem=sems.at[landed],
             device_id=device, device_id_type=MESH,
         )
+
+    def wait_sent(ref, sems, sent):
+        remote(ref, ref, sems, sent, sent, (ep, mate)).wait_send()
+
+    def wait_landed(ref, sems, landed):
+        remote(ref, ref, sems, landed, landed, (ep, mate)).wait_recv()
 
     loads = [
         pltpu.make_async_copy(source, target, sem_in.at[i])
@@ -199,10 +205,15 @@
     for load in loads:
         load.start()
     barrier = pltpu.get_barrier_semaphore()
-    for d in range(1, peers):
-        pl.semaphore_signal(barrier, inc=1, device_id=(peer[d], tp), device_id_type=MESH)
-    pl.semaphore_signal(barrier, inc=1, device_id=(ep, mate), device_id_type=MESH)
-    pl.semaphore_signal(barrier, inc=1, device_id=(ep, across), device_id_type=MESH)
+    for device in [(peer[d], tp) for d in range(1, half)] + [(ep, mate), (ep, across)]:
+        pl.semaphore_signal(barrier, inc=1, device_id=device, device_id_type=MESH)
+
+    @pl.when(is_inner)
+    def _():
+        for far in (2, 3):
+            device = (2 * layers[far] + column, tp)
+            pl.semaphore_signal(barrier, inc=1, device_id=device, device_id_type=MESH)
+
     loads[0].wait()
     loads[1].wait()
 
@@ -219,114 +230,97 @@
     loads[2].wait()
     loads[3].wait()
     with jax.named_scope("barrier"):
-        pl.semaphore_wait(barrier, peers + 1)
+        pl.semaphore_wait(barrier, half + 2)
 
     own = gather[block(side_of, half * cap)]
-    send_e = remote(experts, cross_e.at[1 - inner], sem_e, 1 - inner, far_gate)
+    send_e = remote(experts, cross_e.at[1 - inner], sem_e, 2, 1 - inner, far_gate)
     send_e.start()
-    copy_w = {}
-    for d in range(1, peers):
-        copy_w[d] = remote(
-            wsend.at[lax.div(peer[d], per_row)], wrecv.at[ep], sem_w, d, (peer[d], tp)
-        )
-        copy_w[d].start()
-    raw_t = remote(tokens, cross_t.at[1 - inner], sem_xt, 1 - inner, far_gate)
-    raw_c = remote(cotangent, cross_c.at[1 - inner], sem_xc, 1 - inner, far_gate)
-
-    raw_t.start()
-    raw_c.start()
-
-    def near_copy(d, packed, landed, sems):
-        return remote(packed.at[block(spot[d])], landed.at[block(ep)], sems, d, (peer[d], tp))
+
+    def send_weights(target, far):
+        remote(
+            wsend.at[lax.div(target, per_row)], wrecv.at[ep], sem_w, 2, far, (target, tp)
+        ).start()
+
+    for d in range(1, half):
+        send_weights(peer[d], 0)
+    remote(tokens, cross_t.at[1 - inner], sem_x, 4, 1 - inner, far_gate).start()
+    remote(cotangent, cross_c.at[1 - inner], sem_x, 4, 3 - inner, far_gate).start()
 
     for source, packed, landed, sems in (
         (tokens, send_t, recv_t, sem_t), (cotangent, send_c, recv_c, sem_c)
     ):
         packed[...] = dot(own, source[...], 1, 0).astype(jnp.bfloat16)
-        for d in (1, 2, 3):
-            near_copy(d, packed, landed, sems).start()
+        for d in range(1, half):
+            remote(
+                packed.at[block(spot[d])], landed.at[block(ep)], sems, 2, min(d - 1, 1), (peer[d], tp)
+            ).start()
         landed[block(ep)] = packed[block(place)]
 
     for load in loads[4:]:
         load.wait()
 
-    def relay_copy(k, d, packed, landed, sems):
-        return remote(
-            packed.at[k, block(spot[d])], landed.at[block(2 * layers[2 + k] + column)],
-            sems, 4 * k + d, (peer[d], tp),
-        )
-
     def relay_table(k):
-        remote(experts, cross_e.at[k], sem_e, k, far_gate).wait_recv()
+        wait_landed(cross_e.at[k], sem_e, k)
         chosen_a, chosen_b = slot_table(
             cross_e[k, 0:1], cross_e[k, 1:2], side_of * half, half * cap, cap
         )
         gather_relay[k] = (chosen_a + chosen_b).astype(jnp.bfloat16)
 
-    def relay(k, source, crossed, packed, landed, sems_in, sems_out):
-        with jax.named_scope("wait_raw"):
-            remote(source, crossed.at[k], sems_in, k, far_gate).wait_recv()
+    def relay(k, landed_in, crossed, packed, landed, sems):
+        wait_landed(crossed.at[k], sem_x, landed_in)
         packed[k] = dot(gather_relay[k], crossed[k], 1, 0).astype(jnp.bfloat16)
-        for d in (2, 3, 1):
-            relay_copy(k, d, packed, landed, sems_out).start()
-        landed[block(2 * layers[2 + k] + column)] = packed[k, block(place)]
+        rows = block(2 * layers[2 + k] + column)
+        for d in range(1, half):
+            remote(packed.at[k, block(spot[d])], landed.at[rows], sems, 2, k, (peer[d], tp)).start()
+        landed[rows] = packed[k, block(place)]
 
     def relay_tokens(k, gate):
-        relay(k, tokens, cross_t, relay_t, recv_t, sem_xt, sem_rt)
+        relay(k, k, cross_t, relay_t, recv_t, sem_rt)
 
     def relay_cots(k, gate):
-        relay(k, cotangent, cross_c, relay_c, recv_c, sem_xc, sem_rc)
-
-    def arrive(j, gate, packed, relayed, landed, near_sems, sems):
-        if j < 2:
-            for d in (2 * j, 2 * j + 1):
-                if d:
-                    near_copy(d, packed, landed, near_sems).wait_recv()
-        else:
-            for d in (1,) if gate else (2, 3):
-                with jax.named_scope("arrive%d" % d):
-                    relay_copy(j - 2, d, relayed, landed, sems).wait_recv()
+        relay(k, 2 + k, cross_c, relay_c, recv_c, sem_rc)
+
+    def arrive(j, gate, landed, near_sems, sems):
+        count = cap if j == 0 or (gate and j > 1) else 2 * cap
+        wait_landed(landed.at[block(0, count)], sems if j > 1 else near_sems, j % 2)
+
+    def weights_out(k, gate):
+        for b in range(2):
+            target = 2 * layers[2 + k] + b
+            send_weights(target, 1)
 
     pairs = peers // 2
 
     def core_copy(i):
         part, landed = (part_t, core_t) if i < pairs else (part_c, core_c)
         j = i % pairs
-        return remote(part.at[j, block(1 - core)], landed.at[j], sem_core, i, (ep, mate))
+        return remote(
+            part.at[j, block(1 - core)], landed.at[j], sem_core, 2 * pairs + i // pairs, i, (ep, mate)
+        )
 
     def pair_copy(i):
         summed, landed = (pair_t, pair_in_t) if i < pairs else (pair_c, pair_in_c)
-        return remote(summed.at[i % pairs], landed.at[i % pairs], sem_pair, i, (ep, across))
+        return remote(
+            summed.at[i % pairs], landed.at[i % pairs], sem_pair, 2 * pairs + i // pairs, i,
+            (ep, across),
+        )
 
     def act_copy(j):
         rows = block(2 * layers[j] + core)
-        return remote(acts.at[rows], acts.at[rows], sem_act, j, (ep, mate))
-
-    def comb_copy(j):
-        source = 2 * layers[j] + core
-        return remote(comb.at[source], comb.at[source], sem_comb, j, (ep, mate))
-
-    def distance(j, b):
-        return 2 * j + b if j < 2 else 4 + 2 * lax.rem(j + inner, 2) + b
-
-    def back_copies(j, b):
-        target = 2 * layers[j] + lax.rem(column + b, 2)
-        return (
-            remote(
-                slot.at[block(target)], ret.at[block(ep)], sem_ret, distance(j, b), (target, tp)
-            ),
-            remote(comb.at[target], comb_ret.at[ep], sem_cret, distance(j, b), (target, tp)),
-        )
+        return remote(acts.at[rows], acts.at[rows], sem_act, pairs, j, (ep, mate))
+
+    def comb_send(source, device):
+        remote(comb.at[source], comb_ret.at[ep], sem_cret, 1, 0, (source, device)).start()
 
     def parts_tokens(j, gate):
-        arrive(j, gate, send_t, relay_t, recv_t, sem_t, sem_rt)
+        arrive(j, gate, recv_t, sem_t, sem_rt)
         rows = recv_t[block(layers[j], 2 * cap)]
         part_t[j, :, :f] = dot(rows, w_gate[...], 1, 0).astype(jnp.bfloat16)
         part_t[j, :, f:] = dot(rows, w_up[...], 1, 0).astype(jnp.bfloat16)
         core_copy(j).start()
 
     def parts_cots(j, gate):
-        arrive(j, gate, send_c, relay_c, recv_c, sem_c, sem_rc)
+        arrive(j, gate, recv_c, sem_c, sem_rc)
         cots = recv_c[block(layers[j], 2 * cap)]
         part_c[j] = dot(cots, w_down[...], 1, 1).astype(jnp.bfloat16)
         core_copy(pairs + j).start()
@@ -345,8 +339,9 @@
 
     def act(j, gate):
         if j == 0:
-            for d in range(1, peers):
-                copy_w[d].wait_recv()
+            wait_landed(wrecv.at[0:half - 1], sem_w, 0)
+        if j == 3:
+            wait_landed(wrecv.at[0:half], sem_w, 1)
         pair_copy(j).wait_recv()
         pair_copy(pairs + j).wait_recv()
         source = 2 * layers[j] + core
@@ -372,21 +367,31 @@
         total = jnp.sum(hidden * grad_scaled, axis=1, keepdims=True)
         wide = jnp.concatenate([jnp.broadcast_to(total, (cap, LANES))] * per_row, axis=0)
         comb[source] = wide.T[:8]
-        comb_copy(j).start()
+        comb_send(source, mate)
+        if j:
+            comb_send(source, tp)
+        else:
+            @pl.when(source == ep)
+            def _():
+                comb_ret[ep] = comb[ep]
+
+            @pl.when(source != ep)
+            def _():
+                comb_send(source, tp)
 
     def slots_back(j, gate):
         act_copy(j).wait_recv()
-        comb_copy(j).wait_recv()
         rows = block(layers[j], 2 * cap)
         value = dot(acts[rows, f:2 * f], w_gate[...], 1, 1) + dot(acts[rows, 2 * f:], w_up[...], 1, 1)
         slot[rows] = value.astype(jnp.bfloat16)
         for b in range(2):
+            target = 2 * layers[j] + lax.rem(column + b, 2)
             if j == b == 0:
                 ret[block(ep)] = slot[block(ep)]
-                comb_ret[ep] = comb[ep]
             else:
-                for copy in back_copies(j, b):
-                    copy.start()
+                remote(
+                    slot.at[block(target)], ret.at[block(ep)], sem_ret, 1, 0, (target, tp)
+                ).start()
 
     def tables(k, gate):
         relay_table(k)
@@ -400,17 +405,19 @@
             up_grad[...] = dot(recv_t[...], acts[:, 2 * f:], 0, 0)
 
     names = {
+        "w": weights_out,
         "T": tables, "rt": relay_tokens, "rc": relay_cots, "pt": parts_tokens, "pc": parts_cots,
         "st": pair_tokens, "sc": pair_cots, "a": act, "b": slots_back, "g": grads,
     }
     outer_order = (
-        "pt0", "pc0", "st0", "sc0", "pt1", "st1", "pc1", "sc1", "a0", "b0", "pt3", "st3",
-        "a1", "b1", "pc3", "sc3", "pt2", "st2", "a3", "b3", "pc2", "sc2", "a2", "b2",
+        "pt0", "st0", "pt1", "w0", "pc0", "sc0", "st1", "pc1", "sc1", "a0", "pt3", "w1",
+        "b0", "st3", "a1", "pc3", "b1", "sc3", "pt2", "st2", "a3", "pc2", "b3", "sc2",
+        "a2", "b2",
     )
     inner_order = (
-        "pt0", "T1", "pc0", "st0", "T0", "sc0", "rt1", "a0", "rc1", "b0", "pt3", "st3",
-        "rt0", "pt1", "st1", "pc3", "sc3", "rc0", "pc1", "sc1", "a3", "pt2", "st2", "a1",
-        "b3", "b1", "pc2", "sc2", "a2", "b2",
+        "pt0", "w0", "T1", "T0", "st0", "pc0", "rt1", "sc0", "rc1", "a0", "pt3", "w1",
+        "rt0", "b0", "st3", "pt1", "rc0", "st1", "pc3", "sc3", "pc1", "pt2", "sc1", "st2",
+        "pc2", "a3", "b3", "sc2", "a1", "b1", "a2", "b2",
     )
     for role, order, gate in ((is_outer, outer_order, False), (is_inner, inner_order, True)):
         @pl.when(role)
@@ -424,8 +431,16 @@
             grads(which, None)
 
     with jax.named_scope("cret"):
-        for d in range(1, peers):
-            remote(comb.at[0], comb_ret.at[0], sem_cret, d, (peer[d], tp)).wait_recv()
+        own_half = core == column
+
+        @pl.when(own_half)
+        def _():
+            wait_landed(comb_ret.at[0:peers - 1], sem_cret, 0)
+
+        @pl.when(jnp.logical_not(own_half))
+        def _():
+            wait_landed(comb_ret, sem_cret, 0)
+
     part_lane = lax.broadcasted_iota(jnp.int32, (1, LANES), 1)
     totals = [jnp.zeros((1, tokens.shape[0]), jnp.float32)] * 2
     for q in range(slots // LANES):
@@ -439,31 +454,34 @@
     for k in range(2):
         grad_combine[k:k + 1] = totals[k]
     with jax.named_scope("ret"):
-        for d in range(1, peers):
-            remote(slot.at[block(0)], ret.at[block(0)], sem_ret, d, (peer[d], tp)).wait_recv()
-    grad_tokens[...] = dot(gather[...], ret[...], 0, 0).astype(jnp.bfloat16)
-    for copy in (send_e, raw_t, raw_c, *copy_w.values()):
-        copy.wait_send()
-    for d in range(1, half):
-        near_copy(d, send_t, recv_t, sem_t).wait_send()
-        near_copy(d, send_c, recv_c, sem_c).wait_send()
-    for j in range(pairs):
-        for copy in (
-            core_copy(j), core_copy(pairs + j), pair_copy(j), pair_copy(pairs + j),
-            act_copy(j), comb_copy(j),
-        ):
-            copy.wait_send()
-        for b in range(2):
-            if j or b:
-                for copy in back_copies(j, b):
-                    copy.wait_send()
-
-    @pl.when(is_inner)
-    def _():
-        for k in range(2):
-            for d in range(1, half):
-                relay_copy(k, d, relay_t, recv_t, sem_rt).wait_send()
-                relay_copy(k, d, relay_c, recv_c, sem_rc).wait_send()
+        wait_landed(ret.at[block(0, (peers - 1) * cap)], sem_ret, 0)
+    with jax.named_scope("fin"):
+        grad_tokens[...] = dot(gather[...], ret[...], 0, 0).astype(jnp.bfloat16)
+    with jax.named_scope("sends"):
+        send_e.wait_send()
+        wait_sent(send_t.at[block(0, (half - 1) * cap)], sem_t, 2)
+        wait_sent(send_c.at[block(0, (half - 1) * cap)], sem_c, 2)
+        wait_sent(cross_t, sem_x, 4)
+        wait_sent(wrecv.at[0:peers - 1], sem_w, 2)
+        wait_sent(core_t, sem_core, 2 * pairs)
+        wait_sent(core_c, sem_core, 2 * pairs + 1)
+        wait_sent(pair_t, sem_pair, 2 * pairs)
+        wait_sent(pair_c, sem_pair, 2 * pairs + 1)
+        wait_sent(acts.at[block(0, pairs * cap)], sem_act, pairs)
+        wait_sent(slot.at[block(0, (peers - 1) * cap)], sem_ret, 1)
+
+        @pl.when(own_half)
+        def _():
+            wait_sent(comb.at[0:peers - 1], sem_cret, 1)
+
+        @pl.when(jnp.logical_not(own_half))
+        def _():
+            wait_sent(comb, sem_cret, 1)
+
+        @pl.when(is_inner)
+        def _():
+            wait_sent(recv_t.at[block(0, 2 * (half - 1) * cap)], sem_rt, 2)
+            wait_sent(recv_t.at[block(0, 2 * (half - 1) * cap)], sem_rc, 2)
 
 
 def store_kernel(count, *refs):
@@ -520,10 +538,8 @@
             pltpu.VMEM((slots, 3 * f), bf16), small, landed, landed,
             small, pltpu.VMEM((slots, count), bf16), pltpu.VMEM((2, slots // 2, count), bf16),
             pltpu.VMEM((picks, slots, count), f32),
-            dma((7,)), dma((2, peers)), dma((2, peers)), dma((2, peers)), dma((2, peers)),
-            dma((2, 2)), dma((2, 2)), dma((2, peers)), dma((2, 2)),
-            dma((2, 2 * pairs)), dma((2, 2 * pairs)), dma((2, pairs)), dma((2, pairs)),
-            dma((2, peers)), dma((2, peers)),
+            dma((7,)), dma((3,)), dma((3,)), dma((3,)), dma((3,)), dma((5,)), dma((3,)), dma((3,)),
+            dma((2 * pairs + 2,)), dma((2 * pairs + 2,)), dma((pairs + 1,)), dma((2,)), dma((2,)),
         ],
         compiler_params=pltpu.CompilerParams(
             collective_id=0, has_side_effects=True, vmem_limit_bytes=48 * 1024 * 1024

time: 43.4 us -> 40.3 us (0.929)
  the two profiles are of different devices: /device:TPU:18 before, /device:TPU:15 now
where the time goes in v2:
time: 40.3 us; the launch traced here: 40.1 us
  Pallas kernels  39.5 us (98%)
  between operations  0.64 us (2%)
    pallas_call x1, Pallas kernels, fused_body(): pl.pallas_call(functools.partial(fused_kernel, peers, parts), out_shape=s...  38.2 us
    pallas_call x1, Pallas kernels, fused_body(): pl.pallas_call(functools.partial(store_kernel, len(outs)), out_shape=shap...  1.23 us

profile of v2, /device:TPU:15, one launch (start us, length us, event | category | flops | bytes accessed | tf_op | source)
XLA Modules:
  0.0 40.1 jit_solution(15035830507251408403)
XLA Ops:
  0.6 38.2 %shard_map.110 = (bf16[128,512]{1,0:T(8,128)(2,1)S(1)}, f32[2,128]{1,0:T(2,128)S(1)}, f32[512,256]{1,0:T(8,128)S(1)}, f32[512,256]{1,0:T(8,128)S(1)}, f32[256,512]{1,0:T(8,128)S(1)}) custom-call(bf16[128,512]{1,0:T(8,128)(2,1)} %tokens_hbm.1, bf16[128,512]{1,0:T(8,128)(2,1)} %cotangent_hbm.1, s32[2,128]{1,0:T(2,128)} %bitcast.6, f32[2,128]{1,0:T(2,128)} %bitcast.7, ...), custom_call_target="tpu_custom_call" | custom-call | tf_op jit(solution)/shard_map/pallas_call | solution.py:525
  38.9 1.2 %shard_map.111 = (bf16[128,512]{1,0:T(8,128)(2,1)}, f32[2,128]{1,0:T(2,128)}, f32[512,256]{1,0:T(8,128)}, f32[512,256]{1,0:T(8,128)}, f32[256,512]{1,0:T(8,128)}) custom-call(bf16[128,512]{1,0:T(8,128)(2,1)S(1)} %get-tuple-element.15.refs_0_, f32[2,128]{1,0:T(2,128)S(1)} %get-tuple-element.16.refs_1_, f32[512,256]{1,0:T(8,128)S(1)} %get-tuple-element.17.refs_2_, ...), custom_call_target="tpu_custom_call" | custom-call | tf_op jit(solution)/shard_map/pallas_call | solution.py:551

commit v3 on v2

--- a/solution.py
+++ b/solution.py
@@ -152,12 +152,12 @@
 
 def fused_kernel(
     peers, parts, tokens_hbm, cotangent_hbm, experts_hbm, combine_hbm, gate_hbm, up_hbm, down_hbm,
-    grad_tokens, grad_combine, gate_grad, up_grad, down_grad,
+    ret, gather, grad_combine, gate_grad, up_grad, down_grad,
     tokens, cotangent, experts, combine, w_gate, w_up, w_down,
     send_t, send_c, cross_t, cross_c, cross_e, relay_t, relay_c, recv_t, recv_c,
     wsend, wrecv, part_t, part_c, core_t, core_c, pair_t, pair_c, pair_in_t, pair_in_c,
-    acts, comb, slot, ret,
-    comb_ret, gather, gather_relay, onehot_k,
+    acts, comb, slot,
+    comb_ret, gather_relay, onehot_k,
     sem_in, sem_t, sem_c, sem_rt, sem_rc, sem_x, sem_w, sem_e,
     sem_core, sem_pair, sem_act, sem_ret, sem_cret,
 ):
@@ -202,8 +202,6 @@
             (down_hbm.at[0], w_down),
         ))
     ]
-    for load in loads:
-        load.start()
     barrier = pltpu.get_barrier_semaphore()
     for device in [(peer[d], tp) for d in range(1, half)] + [(ep, mate), (ep, across)]:
         pl.semaphore_signal(barrier, inc=1, device_id=device, device_id_type=MESH)
@@ -214,6 +212,8 @@
             device = (2 * layers[far] + column, tp)
             pl.semaphore_signal(barrier, inc=1, device_id=device, device_id_type=MESH)
 
+    for load in loads:
+        load.start()
     loads[0].wait()
     loads[1].wait()
 
@@ -229,10 +229,12 @@
     wrecv[ep] = wsend[lax.div(ep, per_row)]
     loads[2].wait()
     loads[3].wait()
+    own = gather[block(side_of, half * cap)]
+    send_t[...] = dot(own, tokens[...], 1, 0).astype(jnp.bfloat16)
+    send_c[...] = dot(own, cotangent[...], 1, 0).astype(jnp.bfloat16)
     with jax.named_scope("barrier"):
         pl.semaphore_wait(barrier, half + 2)
 
-    own = gather[block(side_of, half * cap)]
     send_e = remote(experts, cross_e.at[1 - inner], sem_e, 2, 1 - inner, far_gate)
     send_e.start()
 
@@ -246,15 +248,16 @@
     remote(tokens, cross_t.at[1 - inner], sem_x, 4, 1 - inner, far_gate).start()
     remote(cotangent, cross_c.at[1 - inner], sem_x, 4, 3 - inner, far_gate).start()
 
-    for source, packed, landed, sems in (
-        (tokens, send_t, recv_t, sem_t), (cotangent, send_c, recv_c, sem_c)
-    ):
-        packed[...] = dot(own, source[...], 1, 0).astype(jnp.bfloat16)
-        for d in range(1, half):
-            remote(
-                packed.at[block(spot[d])], landed.at[block(ep)], sems, 2, min(d - 1, 1), (peer[d], tp)
-            ).start()
-        landed[block(ep)] = packed[block(place)]
+    def near_send(k, d):
+        packed, landed, sems = ((send_t, recv_t, sem_t), (send_c, recv_c, sem_c))[k]
+        remote(
+            packed.at[block(spot[d])], landed.at[block(ep)], sems, 2, min(d - 1, 1), (peer[d], tp)
+        ).start()
+
+    near_send(0, 1)
+    near_send(1, 1)
+    recv_t[block(ep)] = send_t[block(place)]
+    recv_c[block(ep)] = send_c[block(place)]
 
     for load in loads[4:]:
         load.wait()
@@ -270,7 +273,7 @@
         wait_landed(crossed.at[k], sem_x, landed_in)
         packed[k] = dot(gather_relay[k], crossed[k], 1, 0).astype(jnp.bfloat16)
         rows = block(2 * layers[2 + k] + column)
-        for d in range(1, half):
+        for d in (1, 2, 3) if k else (1, 3, 2):
             remote(packed.at[k, block(spot[d])], landed.at[rows], sems, 2, k, (peer[d], tp)).start()
         landed[rows] = packed[k, block(place)]
 
@@ -379,19 +382,30 @@
             def _():
                 comb_send(source, tp)
 
-    def slots_back(j, gate):
-        act_copy(j).wait_recv()
-        rows = block(layers[j], 2 * cap)
+    def slot_rows(j, half_of):
+        source = 2 * layers[j] + half_of
+        rows = block(source)
         value = dot(acts[rows, f:2 * f], w_gate[...], 1, 1) + dot(acts[rows, 2 * f:], w_up[...], 1, 1)
         slot[rows] = value.astype(jnp.bfloat16)
-        for b in range(2):
-            target = 2 * layers[j] + lax.rem(column + b, 2)
-            if j == b == 0:
-                ret[block(ep)] = slot[block(ep)]
-            else:
-                remote(
-                    slot.at[block(target)], ret.at[block(ep)], sem_ret, 1, 0, (target, tp)
-                ).start()
+
+        def send():
+            remote(slot.at[rows], ret.at[block(ep)], sem_ret, 1, 0, (source, tp)).start()
+
+        if j:
+            send()
+        else:
+            pl.when(source != ep)(send)
+
+            @pl.when(source == ep)
+            def _():
+                ret[block(ep)] = slot[rows]
+
+    def slots_own(j, gate):
+        slot_rows(j, core)
+
+    def slots_mate(j, gate):
+        act_copy(j).wait_recv()
+        slot_rows(j, 1 - core)
 
     def tables(k, gate):
         relay_table(k)
@@ -404,20 +418,27 @@
         else:
             up_grad[...] = dot(recv_t[...], acts[:, 2 * f:], 0, 0)
 
+    def near_sends(k, gate):
+        for d in range(half - 1, 1, -1):
+            near_send(k, d)
+
     names = {
+        "n": near_sends,
         "w": weights_out,
         "T": tables, "rt": relay_tokens, "rc": relay_cots, "pt": parts_tokens, "pc": parts_cots,
-        "st": pair_tokens, "sc": pair_cots, "a": act, "b": slots_back, "g": grads,
+        "st": pair_tokens, "sc": pair_cots, "a": act, "o": slots_own, "b": slots_mate,
+        "g": grads,
     }
     outer_order = (
-        "pt0", "st0", "pt1", "w0", "pc0", "sc0", "st1", "pc1", "sc1", "a0", "pt3", "w1",
-        "b0", "st3", "a1", "pc3", "b1", "sc3", "pt2", "st2", "a3", "pc2", "b3", "sc2",
-        "a2", "b2",
+        "n0", "n1", "pt0", "st0", "pt1", "w0", "pc0", "sc0", "st1", "pc1", "sc1", "a0",
+        "o0", "pt3", "w1", "st3", "b0", "pc3", "a1", "o1", "sc3", "b1", "pt2", "st2",
+        "a3", "o3", "pc2", "b3", "sc2", "a2", "o2", "b2",
     )
     inner_order = (
-        "pt0", "w0", "T1", "T0", "st0", "pc0", "rt1", "sc0", "rc1", "a0", "pt3", "w1",
-        "rt0", "b0", "st3", "pt1", "rc0", "st1", "pc3", "sc3", "pc1", "pt2", "sc1", "st2",
-        "pc2", "a3", "b3", "sc2", "a1", "b1", "a2", "b2",
+        "n0", "n1", "pt0", "w0", "T1", "T0", "st0", "pc0", "rt1", "sc0", "rc1", "a0",
+        "o0", "pt3", "w1", "st3", "rt0", "b0", "rc0", "pc3", "sc3", "pt1", "st1", "pt2",
+        "st2", "pc1", "a3", "o3", "sc1", "pc2", "b3", "sc2", "a1", "o1", "a2", "o2",
+        "b1", "b2",
     )
     for role, order, gate in ((is_outer, outer_order, False), (is_inner, inner_order, True)):
         @pl.when(role)
@@ -455,8 +476,6 @@
         grad_combine[k:k + 1] = totals[k]
     with jax.named_scope("ret"):
         wait_landed(ret.at[block(0, (peers - 1) * cap)], sem_ret, 0)
-    with jax.named_scope("fin"):
-        grad_tokens[...] = dot(gather[...], ret[...], 0, 0).astype(jnp.bfloat16)
     with jax.named_scope("sends"):
         send_e.wait_send()
         wait_sent(send_t.at[block(0, (half - 1) * cap)], sem_t, 2)
@@ -484,14 +503,18 @@
             wait_sent(recv_t.at[block(0, 2 * (half - 1) * cap)], sem_rc, 2)
 
 
-def store_kernel(count, *refs):
-    sources, targets, sems = refs[:count], refs[count:2 * count], refs[2 * count]
+def store_kernel(ret, gather, *refs):
+    count = (len(refs) - 2) // 2
+    sources, first, targets = refs[:count], refs[count], refs[count + 1:2 * count + 1]
+    grad_tokens, sems = refs[-2:]
     copies = [
         pltpu.make_async_copy(source, target, sems.at[i])
-        for i, (source, target) in enumerate(zip(sources, targets))
+        for i, (source, target) in enumerate(zip((*sources, grad_tokens), (*targets, first)))
     ]
-    for copy in copies:
+    for copy in copies[:count]:
         copy.start()
+    grad_tokens[...] = dot(gather[...], ret[...], 0, 0).astype(jnp.bfloat16)
+    copies[count].start()
     for copy in copies:
         copy.wait()
 
@@ -524,9 +547,12 @@
     small = pltpu.VMEM((peers, 8, LANES), f32)
     outs = pl.pallas_call(
         functools.partial(fused_kernel, peers, parts),
-        out_shape=shapes,
+        out_shape=(
+            jax.ShapeDtypeStruct((slots, width), bf16), jax.ShapeDtypeStruct((slots, count), bf16),
+            *shapes[1:],
+        ),
         in_specs=[hbm] * 7,
-        out_specs=(vmem,) * 5,
+        out_specs=(vmem,) * 6,
         scratch_shapes=[
             rows, rows, pltpu.VMEM((picks, count), jnp.int32), pltpu.VMEM((picks, count), f32),
             pltpu.VMEM((width, f), bf16), pltpu.VMEM((width, f), bf16), pltpu.VMEM((f, width), bf16),
@@ -535,8 +561,8 @@
             pltpu.VMEM((slots // LANES, 8, LANES), f32), small,
             pltpu.VMEM((pairs, 2 * cap, 2 * f), bf16), pltpu.VMEM((pairs, 2 * cap, f), bf16),
             sums_t, sums_c, sums_t, sums_c, sums_t, sums_c,
-            pltpu.VMEM((slots, 3 * f), bf16), small, landed, landed,
-            small, pltpu.VMEM((slots, count), bf16), pltpu.VMEM((2, slots // 2, count), bf16),
+            pltpu.VMEM((slots, 3 * f), bf16), small, landed,
+            small, pltpu.VMEM((2, slots // 2, count), bf16),
             pltpu.VMEM((picks, slots, count), f32),
             dma((7,)), dma((3,)), dma((3,)), dma((3,)), dma((3,)), dma((5,)), dma((3,)), dma((3,)),
             dma((2 * pairs + 2,)), dma((2 * pairs + 2,)), dma((pairs + 1,)), dma((2,)), dma((2,)),
@@ -549,12 +575,12 @@
         for x in (tokens, cotangent, experts.T, combine.T, w_gate, w_up, w_down)
     ))
     outs = pl.pallas_call(
-        functools.partial(store_kernel, len(outs)),
+        store_kernel,
         out_shape=shapes,
-        in_specs=[vmem] * 5,
+        in_specs=[vmem] * 6,
         out_specs=(hbm,) * 5,
-        scratch_shapes=[dma((5,))],
-        compiler_params=pltpu.CompilerParams(vmem_limit_bytes=1024 * 1024),
+        scratch_shapes=[rows, dma((5,))],
+        compiler_params=pltpu.CompilerParams(vmem_limit_bytes=4 * 1024 * 1024),
     )(*outs)
     return outs[0], outs[1].T, outs[2][None], outs[3][None], outs[4][None]
 

time: 40.3 us -> 37.6 us (0.933)
  the two profiles are of different devices: /device:TPU:15 before, /device:TPU:18 now
where the time goes in v3:
time: 37.6 us; the launch traced here: 37.1 us
  Pallas kernels  36.5 us (97%)
  between operations  0.64 us (2%)
    pallas_call x1, Pallas kernels, fused_body(): pl.pallas_call(functools.partial(fused_kernel, peers, parts), out_shape=(...  35.3 us
    pallas_call x1, Pallas kernels, fused_body(): pl.pallas_call(store_kernel, out_shape=shapes, in_specs=[vmem] * 6, out_s...  1.22 us

profile of v3, /device:TPU:18, one launch (start us, length us, event | category | flops | bytes accessed | tf_op | source)
XLA Modules:
  0.0 37.1 jit_solution(12037926663779727781)
XLA Ops:
  0.6 35.3 %shard_map.110 = (bf16[512,512]{1,0:T(8,128)(2,1)S(1)}, bf16[512,128]{1,0:T(8,128)(2,1)S(1)}, f32[2,128]{1,0:T(2,128)S(1)}, f32[512,256]{1,0:T(8,128)S(1)}, f32[...) custom-call(bf16[128,512]{1,0:T(8,128)(2,1)} %tokens_hbm.1, bf16[128,512]{1,0:T(8,128)(2,1)} %cotangent_hbm.1, ...), custom_call_target="tpu_custom_call" | custom-call | tf_op jit(solution)/shard_map/pallas_call | solution.py:548
  35.9 1.2 %shard_map.111 = (bf16[128,512]{1,0:T(8,128)(2,1)}, f32[2,128]{1,0:T(2,128)}, f32[512,256]{1,0:T(8,128)}, f32[512,256]{1,0:T(8,128)}, f32[256,512]{1,0:T(8,128)}) custom-call(bf16[512,512]{1,0:T(8,128)(2,1)S(1)} %get-tuple-element.16.ret, bf16[512,128]{1,0:T(8,128)(2,1)S(1)} %get-tuple-element.17.gather, f32[2,128]{1,0:T(2,128)S(1)} %get-tuple-element.18.refs_0_, ...), custom_call_target="tpu_custom_call" | custom-call | tf_op jit(solution)/shard_map/pallas_call | solution.py:577

commit v4 on v3

--- a/solution.py
+++ b/solution.py
@@ -153,7 +153,7 @@
 def fused_kernel(
     peers, parts, tokens_hbm, cotangent_hbm, experts_hbm, combine_hbm, gate_hbm, up_hbm, down_hbm,
     ret, gather, grad_combine, gate_grad, up_grad, down_grad,
-    tokens, cotangent, experts, combine, w_gate, w_up, w_down,
+    tokens, cotangent, experts, combine, w_gate, w_up, w_down, w_slot, w_part,
     send_t, send_c, cross_t, cross_c, cross_e, relay_t, relay_c, recv_t, recv_c,
     wsend, wrecv, part_t, part_c, core_t, core_c, pair_t, pair_c, pair_in_t, pair_in_c,
     acts, comb, slot,
@@ -261,6 +261,10 @@
 
     for load in loads[4:]:
         load.wait()
+    with jax.named_scope("transposes"):
+        w_slot[:f] = w_gate[...].T
+        w_slot[f:] = w_up[...].T
+        w_part[...] = w_down[...].T
 
     def relay_table(k):
         wait_landed(cross_e.at[k], sem_e, k)
@@ -325,7 +329,7 @@
     def parts_cots(j, gate):
         arrive(j, gate, recv_c, sem_c, sem_rc)
         cots = recv_c[block(layers[j], 2 * cap)]
-        part_c[j] = dot(cots, w_down[...], 1, 1).astype(jnp.bfloat16)
+        part_c[j] = dot(cots, w_part[...], 1, 0).astype(jnp.bfloat16)
         core_copy(pairs + j).start()
 
     def pair_sum(j, i, part, landed, summed):
@@ -385,8 +389,7 @@
     def slot_rows(j, half_of):
         source = 2 * layers[j] + half_of
         rows = block(source)
-        value = dot(acts[rows, f:2 * f], w_gate[...], 1, 1) + dot(acts[rows, 2 * f:], w_up[...], 1, 1)
-        slot[rows] = value.astype(jnp.bfloat16)
+        slot[rows] = dot(acts[rows, f:], w_slot[...], 1, 0).astype(jnp.bfloat16)
 
         def send():
             remote(slot.at[rows], ret.at[block(ep)], sem_ret, 1, 0, (source, tp)).start()
@@ -431,16 +434,27 @@
     }
     outer_order = (
         "n0", "n1", "pt0", "st0", "pt1", "w0", "pc0", "sc0", "st1", "pc1", "sc1", "a0",
-        "o0", "pt3", "w1", "st3", "b0", "pc3", "a1", "o1", "sc3", "b1", "pt2", "st2",
-        "a3", "o3", "pc2", "b3", "sc2", "a2", "o2", "b2",
-    )
-    inner_order = (
+        "o0", "pt3", "w1", "st3", "b0", "pc3", "a1", "o1", "sc3", "b1", "pt2", "a3",
+        "o3", "st2", "pc2", "sc2", "b3", "a2", "o2", "b2",
+    )
+    inner_low = (
+        "n0", "n1", "pt0", "w0", "T1", "T0", "st0", "pc0", "rt1", "sc0", "rc1", "a0",
+        "o0", "rt0", "pt3", "w1", "rc0", "st3", "b0", "pc3", "sc3", "pt1", "st1", "pt2",
+        "st2", "pc1", "a3", "o3", "sc1", "pc2", "b3", "sc2", "a1", "o1", "a2", "o2",
+        "b1", "b2",
+    )
+    inner_high = (
         "n0", "n1", "pt0", "w0", "T1", "T0", "st0", "pc0", "rt1", "sc0", "rc1", "a0",
         "o0", "pt3", "w1", "st3", "rt0", "b0", "rc0", "pc3", "sc3", "pt1", "st1", "pt2",
-        "st2", "pc1", "a3", "o3", "sc1", "pc2", "b3", "sc2", "a1", "o1", "a2", "o2",
+        "st2", "pc1", "a3", "o3", "b3", "pc2", "sc1", "sc2", "a1", "o1", "a2", "o2",
         "b1", "b2",
     )
-    for role, order, gate in ((is_outer, outer_order, False), (is_inner, inner_order, True)):
+    for low, order, gate in (
+        (True, outer_order, False), (False, outer_order, False), (True, inner_low, True),
+        (False, inner_high, True),
+    ):
+        role = jnp.logical_and(is_inner if gate else is_outer, side_of == (0 if low else 1))
+
         @pl.when(role)
         def _():
             for word in order:
@@ -556,6 +570,7 @@
         scratch_shapes=[
             rows, rows, pltpu.VMEM((picks, count), jnp.int32), pltpu.VMEM((picks, count), f32),
             pltpu.VMEM((width, f), bf16), pltpu.VMEM((width, f), bf16), pltpu.VMEM((f, width), bf16),
+            pltpu.VMEM((2 * f, width), bf16), pltpu.VMEM((width, f), bf16),
             half_rows, half_rows, crossed, crossed, pltpu.VMEM((2, picks, count), jnp.int32),
             relayed, relayed, landed, landed,
             pltpu.VMEM((slots // LANES, 8, LANES), f32), small,

time: 37.6 us -> 37.4 us (level)
  no operation moved by 1% of the time
where the time goes in v4:
time: 37.4 us; the launch traced here: 37.3 us
  Pallas kernels  36.6 us (98%)
  between operations  0.64 us (2%)
    pallas_call x1, Pallas kernels, fused_body(): pl.pallas_call(functools.partial(fused_kernel, peers, parts), out_shape=(...  35.4 us
    pallas_call x1, Pallas kernels, fused_body(): pl.pallas_call(store_kernel, out_shape=shapes, in_specs=[vmem] * 6, out_s...  1.22 us

profile of v4, /device:TPU:18, one launch (start us, length us, event | category | flops | bytes accessed | tf_op | source)
XLA Modules:
  0.0 37.3 jit_solution(4899817321265044110)
XLA Ops:
  0.6 35.4 %shard_map.110 = (bf16[512,512]{1,0:T(8,128)(2,1)S(1)}, bf16[512,128]{1,0:T(8,128)(2,1)S(1)}, f32[2,128]{1,0:T(2,128)S(1)}, f32[512,256]{1,0:T(8,128)S(1)}, f32[...) custom-call(bf16[128,512]{1,0:T(8,128)(2,1)} %tokens_hbm.1, bf16[128,512]{1,0:T(8,128)(2,1)} %cotangent_hbm.1, ...), custom_call_target="tpu_custom_call" | custom-call | tf_op jit(solution)/shard_map/pallas_call | solution.py:562
  36.0 1.2 %shard_map.111 = (bf16[128,512]{1,0:T(8,128)(2,1)}, f32[2,128]{1,0:T(2,128)}, f32[512,256]{1,0:T(8,128)}, f32[512,256]{1,0:T(8,128)}, f32[256,512]{1,0:T(8,128)}) custom-call(bf16[512,512]{1,0:T(8,128)(2,1)S(1)} %get-tuple-element.16.ret, bf16[512,128]{1,0:T(8,128)(2,1)S(1)} %get-tuple-element.17.gather, f32[2,128]{1,0:T(2,128)S(1)} %get-tuple-element.18.refs_0_, ...), custom_call_target="tpu_custom_call" | custom-call | tf_op jit(solution)/shard_map/pallas_call | solution.py:592

commit v5 on v4

--- a/solution.py
+++ b/solution.py
@@ -195,7 +195,7 @@
         remote(ref, ref, sems, landed, landed, (ep, mate)).wait_recv()
 
     loads = [
-        pltpu.make_async_copy(source, target, sem_in.at[i])
+        pltpu.make_async_copy(source, target, sem_in.at[max(i // 2, i - 2)])
         for i, (source, target) in enumerate((
             (experts_hbm, experts), (combine_hbm, combine), (tokens_hbm, tokens),
             (cotangent_hbm, cotangent), (gate_hbm.at[0], w_gate), (up_hbm.at[0], w_up),
@@ -214,8 +214,7 @@
 
     for load in loads:
         load.start()
-    loads[0].wait()
-    loads[1].wait()
+    wait_landed(cross_e, sem_in, 0)
 
     first, second = slot_table(experts[0:1], experts[1:2], 0, slots, cap)
     onehot_k[0] = first
@@ -227,8 +226,7 @@
         wide = jnp.broadcast_to(weight_column[q * LANES:(q + 1) * LANES], (LANES, LANES))
         wsend[q] = wide.T[:8]
     wrecv[ep] = wsend[lax.div(ep, per_row)]
-    loads[2].wait()
-    loads[3].wait()
+    wait_landed(cross_t, sem_in, 1)
     own = gather[block(side_of, half * cap)]
     send_t[...] = dot(own, tokens[...], 1, 0).astype(jnp.bfloat16)
     send_c[...] = dot(own, cotangent[...], 1, 0).astype(jnp.bfloat16)
@@ -302,13 +300,13 @@
         part, landed = (part_t, core_t) if i < pairs else (part_c, core_c)
         j = i % pairs
         return remote(
-            part.at[j, block(1 - core)], landed.at[j], sem_core, 2 * pairs + i // pairs, i, (ep, mate)
+            part.at[j, block(1 - core)], landed.at[j], sem_core, 2 * pairs, i, (ep, mate)
         )
 
     def pair_copy(i):
         summed, landed = (pair_t, pair_in_t) if i < pairs else (pair_c, pair_in_c)
         return remote(
-            summed.at[i % pairs], landed.at[i % pairs], sem_pair, 2 * pairs + i // pairs, i,
+            summed.at[i % pairs], landed.at[i % pairs], sem_pair, 2 * pairs, i,
             (ep, across),
         )
 
@@ -496,10 +494,8 @@
         wait_sent(send_c.at[block(0, (half - 1) * cap)], sem_c, 2)
         wait_sent(cross_t, sem_x, 4)
         wait_sent(wrecv.at[0:peers - 1], sem_w, 2)
-        wait_sent(core_t, sem_core, 2 * pairs)
-        wait_sent(core_c, sem_core, 2 * pairs + 1)
-        wait_sent(pair_t, sem_pair, 2 * pairs)
-        wait_sent(pair_c, sem_pair, 2 * pairs + 1)
+        wait_sent(acts.at[block(0, pairs * cap)], sem_core, 2 * pairs)
+        wait_sent(acts.at[block(0, pairs * cap)], sem_pair, 2 * pairs)
         wait_sent(acts.at[block(0, pairs * cap)], sem_act, pairs)
         wait_sent(slot.at[block(0, (peers - 1) * cap)], sem_ret, 1)
 
@@ -579,8 +575,8 @@
             pltpu.VMEM((slots, 3 * f), bf16), small, landed,
             small, pltpu.VMEM((2, slots // 2, count), bf16),
             pltpu.VMEM((picks, slots, count), f32),
-            dma((7,)), dma((3,)), dma((3,)), dma((3,)), dma((3,)), dma((5,)), dma((3,)), dma((3,)),
-            dma((2 * pairs + 2,)), dma((2 * pairs + 2,)), dma((pairs + 1,)), dma((2,)), dma((2,)),
+            dma((5,)), dma((3,)), dma((3,)), dma((3,)), dma((3,)), dma((5,)), dma((3,)), dma((3,)),
+            dma((2 * pairs + 1,)), dma((2 * pairs + 1,)), dma((pairs + 1,)), dma((2,)), dma((2,)),
         ],
         compiler_params=pltpu.CompilerParams(
             collective_id=0, has_side_effects=True, vmem_limit_bytes=48 * 1024 * 1024

time: 37.4 us -> 37.4 us (level)
  no operation moved by 1% of the time
where the time goes in v5:
time: 37.4 us; the launch traced here: 37.2 us
  Pallas kernels  36.6 us (98%)
  between operations  0.64 us (2%)
    pallas_call x1, Pallas kernels, fused_body(): pl.pallas_call(functools.partial(fused_kernel, peers, parts), out_shape=(...  35.3 us
    pallas_call x1, Pallas kernels, fused_body(): pl.pallas_call(store_kernel, out_shape=shapes, in_specs=[vmem] * 6, out_s...  1.22 us

profile of v5, /device:TPU:18, one launch (start us, length us, event | category | flops | bytes accessed | tf_op | source)
XLA Modules:
  0.0 37.2 jit_solution(7788530284891916730)
XLA Ops:
  0.6 35.3 %shard_map.110 = (bf16[512,512]{1,0:T(8,128)(2,1)S(1)}, bf16[512,128]{1,0:T(8,128)(2,1)S(1)}, f32[2,128]{1,0:T(2,128)S(1)}, f32[512,256]{1,0:T(8,128)S(1)}, f32[...) custom-call(bf16[128,512]{1,0:T(8,128)(2,1)} %tokens_hbm.1, bf16[128,512]{1,0:T(8,128)(2,1)} %cotangent_hbm.1, ...), custom_call_target="tpu_custom_call" | custom-call | tf_op jit(solution)/shard_map/pallas_call | solution.py:558
  36.0 1.2 %shard_map.111 = (bf16[128,512]{1,0:T(8,128)(2,1)}, f32[2,128]{1,0:T(2,128)}, f32[512,256]{1,0:T(8,128)}, f32[512,256]{1,0:T(8,128)}, f32[256,512]{1,0:T(8,128)}) custom-call(bf16[512,512]{1,0:T(8,128)(2,1)S(1)} %get-tuple-element.16.ret, bf16[512,128]{1,0:T(8,128)(2,1)S(1)} %get-tuple-element.17.gather, f32[2,128]{1,0:T(2,128)S(1)} %get-tuple-element.18.refs_0_, ...), custom_call_target="tpu_custom_call" | custom-call | tf_op jit(solution)/shard_map/pallas_call | solution.py:588
